TPU v7x, 128 devices: a whole 4x4x4 slice. The times are simulated.
128 devices in a mesh: ep: 64 (over z, y, x), tp: 2 (over core).
Axes of the slice: x: 4, y: 4, z: 4, core: 2. Of those that a mesh axis runs over, the one named last changes fastest.
Arguments:
- inputs: bfloat16 [4096, 2048], P('ep'), may hold values from -6 to 6
- cache_keys: bfloat16 [4096, 2, 64, 1024], P('ep', 'tp'), may hold values from -6 to 6
- cache_values: bfloat16 [4096, 2, 64, 1024], P('ep', 'tp'), may hold values from -12 to 12
- lengths: int32 [4096], P('ep'), may hold values from 1 to 1024, as said below
- query_weight: bfloat16 [2048, 1024], P(None, 'tp'), may hold values from -0.125 to 0.125
- key_weight: bfloat16 [2048, 128], P(None, 'tp'), may hold values from -0.125 to 0.125
- value_weight: bfloat16 [2048, 128], P(None, 'tp'), may hold values from -0.125 to 0.125
- head_bias: float32 [16], P('tp'), may hold values from -7 to -3
- out_weight: bfloat16 [1024, 2048], P('tp'), may hold values from -0.75 to 0.75
- attend_gain: float32 [2048], replicated, may hold values from 0.1 to 1.9
- router_weight: bfloat16 [2048, 64], replicated, may hold values from -0.125 to 0.125
- routes: int32 [4096, 4], P('ep'), may hold values from 0 to 63, all different within a row; in each aligned block of 64 rows (0 to 63, 64 to 127, ...) at most 8 rows name the same one
- expert_gate: bfloat16 [64, 2048, 512], P('ep', None, 'tp'), may hold values from -0.125 to 0.125
- expert_up: bfloat16 [64, 2048, 512], P('ep', None, 'tp'), may hold values from -0.125 to 0.125
- expert_down: bfloat16 [64, 512, 2048], P('ep', 'tp'), may hold values from -0.25 to 0.25
- shared_gate: bfloat16 [2048, 512], P(None, 'tp'), may hold values from -0.125 to 0.125
- shared_up: bfloat16 [2048, 512], P(None, 'tp'), may hold values from -0.125 to 0.125
- shared_down: bfloat16 [512, 2048], P('tp'), may hold values from -0.25 to 0.25
- final_gain: float32 [2048], P('tp'), may hold values from 0.1 to 1.9
Outputs:
- output: bfloat16 [4096, 2048], P('ep', 'tp')
- new_keys: bfloat16 [4096, 128], P('ep', 'tp')
- new_values: bfloat16 [4096, 128], P('ep', 'tp')
Inputs may be any that keep to these rules, and one draw needn't show every extreme that they name: `lengths`: some sequence has 1024 filled positions and some other has 1. `routes`: each row names 4 different experts. Among the 64 rows of one index of ep no expert is named more than 8 times; some expert is named exactly 8 times by the rows of some index.
All inputs are finite; a program needn't handle non-finite values.
Results may differ from a plain program's by a relative error of at most 0.015.
Values may be sent and summed in bfloat16 or wider, within the bound.
No kernel may reach another device: no remote copies, remote signals or barrier semaphores. Data moves between devices by JAX's collectives and lax.ppermute only.
A program may use at most 128 MiB of HBM per device.

v0:
```python
import math

import jax
import jax.numpy as jnp
from jax import lax
from jax.sharding import PartitionSpec as P

RESIDUAL_SCALE = 2.0**0.25
ROUTE_SCALE = 2.5
NORM_EPS = 1e-05


def sent_to_all(x, axis):
    length = lax.axis_size(axis)
    return lax.all_to_all(jnp.broadcast_to(x[None], (length, *x.shape)), axis, 0, 0, tiled=True)


def over_copies(x, axis):
    return sent_to_all(x, axis).astype(jnp.float32).sum(axis=0)


def laid_out(tiles, dim):
    dims = list(tiles.shape[1:])
    dims[dim] *= tiles.shape[0]
    return jnp.moveaxis(tiles, 0, dim).reshape(dims)


def gather_directly(x, axis, dim):
    return laid_out(sent_to_all(x, axis), dim)


def cut_along(x, dim, length):
    dims = x.shape
    tiles = x.reshape(*dims[:dim], length, dims[dim] // length, *dims[dim + 1 :])
    return jnp.moveaxis(tiles, dim, 0)


def summed_on_arrival(x, axis, dim):
    tiles = cut_along(x, dim, lax.axis_size(axis))
    arrived = lax.all_to_all(tiles, axis, split_axis=0, concat_axis=0, tiled=True)
    return arrived.astype(jnp.float32).sum(axis=0)


def layer_norm(values, gain_vec):
    row_mean = jnp.mean(values, axis=-1, keepdims=True)
    centered = values - row_mean
    row_var = jnp.mean(centered * centered, axis=-1, keepdims=True)
    return centered * lax.rsqrt(row_var + NORM_EPS) * gain_vec


def strictly_later(size):
    row_pos = lax.broadcasted_iota(jnp.int32, (size, size), 0)
    col_pos = lax.broadcasted_iota(jnp.int32, (size, size), 1)
    return (row_pos > col_pos).astype(jnp.float32)


def later_totals(log_keep):
    lead = log_keep.shape[:-1]
    length = log_keep.shape[-1]
    block_size = math.gcd(length, 128)
    block_count = length // block_size
    blocked = log_keep.reshape(lead + (block_count, block_size))
    inside = jnp.einsum("...bi,ic->...bc", blocked, strictly_later(block_size))
    block_total = jnp.sum(blocked, axis=-1)
    after = jnp.einsum("...i,ic->...c", block_total, strictly_later(block_count))
    return (inside + after[..., None]).reshape(lead + (length,))


def on_device(
    inputs,
    cache_keys,
    cache_values,
    lengths,
    query_weight,
    key_weight,
    value_weight,
    head_bias,
    out_weight,
    attend_gain,
    router_weight,
    routes,
    expert_gate,
    expert_up,
    expert_down,
    shared_gate,
    shared_up,
    shared_down,
    final_gain,
):
    seq_count, model_width = inputs.shape
    key_heads, head_size, cache_length = cache_keys.shape[1:]
    query_heads = head_bias.shape[0]
    groups = query_heads // key_heads
    choices_count = routes.shape[1]
    experts = router_weight.shape[1]
    core_index = lax.axis_index("tp")
    half_width = model_width // lax.axis_size("tp")
    query = jnp.dot(inputs, query_weight, preferred_element_type=jnp.float32).astype(jnp.bfloat16)
    query = query.reshape(seq_count, key_heads, groups, head_size)
    new_keys = jnp.dot(inputs, key_weight, preferred_element_type=jnp.float32).astype(jnp.bfloat16)
    new_values = jnp.dot(inputs, value_weight, preferred_element_type=jnp.float32).astype(
        jnp.bfloat16
    )
    scores = jnp.einsum("skgd,skdc->skgc", query, cache_keys, preferred_element_type=jnp.float32)
    scores = scores * head_size ** (-0.5) + head_bias.reshape(key_heads, groups)[None, :, :, None]
    usable = (
        lax.broadcasted_iota(jnp.int32, (1, 1, 1, cache_length), 3) < lengths[:, None, None, None]
    )
    log_keep = jnp.where(usable, jax.nn.log_sigmoid(-scores), 0.0)
    later_sum = later_totals(log_keep)
    stick_weight = jnp.where(usable, jnp.exp(jax.nn.log_sigmoid(scores) + later_sum), 0.0).astype(
        jnp.bfloat16
    )
    attended = jnp.einsum(
        "skgc,skdc->skgd", stick_weight, cache_values, preferred_element_type=jnp.float32
    )
    attended = attended.astype(jnp.bfloat16).reshape(seq_count, query_heads * head_size)
    attention = over_copies(
        jnp.dot(attended, out_weight, preferred_element_type=jnp.float32).astype(jnp.bfloat16), "tp"
    ).astype(jnp.float32)
    hidden = layer_norm(
        RESIDUAL_SCALE * inputs.astype(jnp.float32) + attention, attend_gain
    ).astype(jnp.bfloat16)
    router_probs = jax.nn.sigmoid(
        jnp.dot(hidden, router_weight, preferred_element_type=jnp.float32)
    )
    picked = routes[:, :, None] == lax.broadcasted_iota(jnp.int32, (1, 1, experts), 2)
    chosen = jnp.sum(jnp.where(picked, router_probs[:, None, :], 0.0), axis=2)
    route_weights = ROUTE_SCALE * chosen / jnp.sum(chosen, axis=1, keepdims=True)
    capacity = 2 * seq_count * choices_count // experts
    row_total = seq_count * choices_count
    onehot_float = picked.reshape(row_total, experts).astype(jnp.float32)
    earlier_count = jnp.dot(strictly_later(row_total), onehot_float)
    slot_index = jnp.sum(earlier_count * onehot_float, axis=1).astype(jnp.int32)
    target = routes.reshape(-1) * capacity + slot_index
    selector_float = (
        target[:, None] == lax.broadcasted_iota(jnp.int32, (1, experts * capacity), 1)
    ).astype(jnp.float32)
    selector = selector_float.astype(jnp.bfloat16)
    placement = jnp.sum(selector_float.reshape(seq_count, choices_count, -1), axis=1).astype(
        jnp.bfloat16
    )
    source = lax.dynamic_slice_in_dim(hidden, core_index * half_width, half_width, 1)
    outgoing = lax.dot_general(
        placement, source, (((0,), (0,)), ((), ())), preferred_element_type=jnp.float32
    )
    outgoing = outgoing.astype(jnp.bfloat16).reshape(experts, capacity, -1)
    arrived = lax.all_to_all(outgoing, "ep", split_axis=0, concat_axis=0, tiled=True)
    senders, slot_count, _ = arrived.shape
    flat_rows = arrived.reshape(senders * slot_count, -1)
    flat_rows = gather_directly(flat_rows, "tp", 1)
    gate_act = jnp.dot(flat_rows, expert_gate[0], preferred_element_type=jnp.float32)
    up_act = jnp.dot(flat_rows, expert_up[0], preferred_element_type=jnp.float32)
    inner = (jax.nn.silu(gate_act) * up_act).astype(jnp.bfloat16)
    partial_value = jnp.dot(inner, expert_down[0], preferred_element_type=jnp.float32)
    summed = summed_on_arrival(partial_value.astype(jnp.bfloat16), "tp", 1)
    back_rows = summed.astype(jnp.bfloat16).reshape(senders, slot_count, -1)
    returned = lax.all_to_all(back_rows, "ep", split_axis=0, concat_axis=0, tiled=True)
    gathered = jnp.dot(
        selector, returned.reshape(experts * capacity, -1), preferred_element_type=jnp.float32
    )
    gathered = gathered.reshape(seq_count, choices_count, -1)
    routed = jnp.sum(route_weights[:, :, None] * gathered, axis=1)
    shared_g = jnp.dot(hidden, shared_gate, preferred_element_type=jnp.float32)
    shared_u = jnp.dot(hidden, shared_up, preferred_element_type=jnp.float32)
    shared_inner = (jax.nn.silu(shared_g) * shared_u).astype(jnp.bfloat16)
    shared_partial = jnp.dot(shared_inner, shared_down, preferred_element_type=jnp.float32)
    shared_result = summed_on_arrival(shared_partial.astype(jnp.bfloat16), "tp", 1)
    own_hidden = lax.dynamic_slice_in_dim(hidden, core_index * half_width, half_width, 1)
    mixed_rows = RESIDUAL_SCALE * own_hidden.astype(jnp.float32) + routed + shared_result
    totals = lax.psum((jnp.sum(mixed_rows, axis=1), jnp.sum(mixed_rows * mixed_rows, axis=1)), "tp")
    row_mean = totals[0] / model_width
    row_var = totals[1] / model_width - row_mean * row_mean
    normed = (mixed_rows - row_mean[:, None]) * lax.rsqrt(row_var + NORM_EPS)[:, None]
    output = (normed * final_gain).astype(jnp.bfloat16)
    return (output, new_keys, new_values)


def solution(mesh):
    placed = (
        P("ep", None),
        P("ep", "tp", None, None),
        P("ep", "tp", None, None),
        P("ep"),
        P(None, "tp"),
        P(None, "tp"),
        P(None, "tp"),
        P("tp"),
        P("tp", None),
        P(),
        P(),
        P("ep", None),
        P("ep", None, "tp"),
        P("ep", None, "tp"),
        P("ep", "tp", None),
        P(None, "tp"),
        P(None, "tp"),
        P("tp", None),
        P("tp"),
    )
    return jax.shard_map(
        on_device,
        mesh=mesh,
        in_specs=placed,
        out_specs=(P("ep", "tp"), P("ep", "tp"), P("ep", "tp")),
        check_vma=False,
    )
```

profile of v0, /device:TPU:1, one launch (start us, length us, event | category | flops | bytes accessed | tf_op | source)
XLA Modules:
  0.0 127.4 jit_solution(8843762472364004527)
XLA Ops:
  0.7 2.3 %convolution_convert_fusion.4 = bf16[64,512]{1,0:T(8,128)(2,1)S(1)} fusion(bf16[64,2048]{1,0:T(8,128)(2,1)} %param.19, bf16[2048,512]{1,0:T(8,128)(2,1)} %param.23), kind=kOutput, calls=%fused_computation.29 | convolution fusion | flops 134250496 | bytes 2424832 | tf_op jit(solution)/shard_map/dot_general | solution.py:98
  3.0 0.1 reshape.209
  3.2 4.6 %fusion.2 = f32[64,8,1024]{2,1,0:T(8,128)S(1)} fusion(bf16[64,8,64]{2,1,0:T(8,128)(2,1)S(1)} %reshape.209, bf16[64,1,64,1024]{3,2,1,0:T(8,128)(2,1)} %param.20), kind=kOutput, calls=%fused_computation.2 | convolution fusion | flops 67108864 | bytes 10551296 | tf_op jit(solution)/shard_map/skgd,skdc->skgc/dot_general | solution.py:104
  7.8 1.4 %copy-done.1 = f32[64,8,1024]{2,1,0:T(8,128)} copy-done((f32[64,8,1024]{2,1,0:T(8,128)}, f32[64,8,1024]{2,1,0:T(8,128)S(1)}, u32[]{:S(2)}) %copy-start.1) | copy-done | bytes 2097176
  9.2 1.8 %fusion.69 = (bf16[64,8,8]{1,2,0:T(8,128)(2,1)S(1)}, bf16[64,8,8,128]{3,1,2,0:T(8,128)(2,1)S(1)}) fusion(f32[8]{0:T(128)S(1)} %copy-done.13, f32[64,8,1024]{2,1,0:T(8,128)S(1)} %fusion.2, pred[64,1024]{1,0:T(8,128)(4,1)S(1)} %iota_compare_fusion.3), kind=kLoop, calls=%fused_computation.103 | loop fusion | flops 6287360 | bytes 3219488 | tf_op jit(solution)/shard_map/reduce_sum | solution.py:64
  11.0 0.1 copy.57
  11.1 0.1 fusion.61
  11.3 0.8 copy.58
  12.1 2.6 %fusion.14 = f32[64,8,8,128]{3,2,1,0:T(8,128)} fusion(bf16[64,8,8,128]{3,1,2,0:T(8,128)(2,1)S(1)} %get-tuple-element.11, f32[64,8,8]{2,1,0:T(8,128)} %copy.58), kind=kOutput, calls=%fused_computation.21 | convolution fusion | flops 134758400 | bytes 3162112 | tf_op jit(solution)/shard_map/...bi,ic->...bc/dot_general | solution.py:63
  14.7 2.7 %reshape.212 = f32[64,8,1024]{2,1,0:T(8,128)} reshape(f32[64,8,8,128]{3,2,1,0:T(8,128)} %fusion.14) | data formatting | bytes 4194304 | tf_op jit(solution)/shard_map/reshape | solution.py:66
  17.4 7.0 %fusion.20 = bf16[64,8,64]{2,1,0:T(8,128)(2,1)S(1)} fusion(bf16[64,1,64,1024]{3,2,1,0:T(8,128)(2,1)} %param.21, f32[64,8,1024]{2,1,0:T(8,128)} %reshape.212, f32[64,8,1024]{2,1,0:T(8,128)} %copy-done.1, f32[8]{0:T(128)S(1)} %copy-done.13, pred[64,1024]{1,0:T(8,128)(4,1)S(1)} %iota_compare_fusion.3), kind=kOutput, calls=%fused_computation.28 | convolution fusion | flops 73957376 | bytes 12714016 | tf_op jit(solution)/shard_map/skgc,skdc->skgd/dot_general | solution.py:114
  24.4 0.1 reshape.214
  24.6 0.5 convolution_convert_fusion.2
  25.1 0.8 broadcast_in_dim.33
  26.0 5.0 %all-to-all-start = ((bf16[2,64,2048]{2,1,0:T(8,128)(2,1)}), bf16[2,64,2048]{2,1,0:T(8,128)(2,1)S(1)}, u32[]{:S(2)}, u32[]{:S(2)}) async-start(bf16[2,64,2048]{2,1,0:T(8,128)(2,1)} %broadcast_in_dim.33), calls=%async_computation | async-start | bytes 1048576 | tf_op jit(solution)/shard_map/all_to_all | solution.py:15
  30.9 1.4 %all-to-all-done = bf16[2,64,2048]{2,1,0:T(8,128)(2,1)S(1)} async-done(((bf16[2,64,2048]{2,1,0:T(8,128)(2,1)}), bf16[2,64,2048]{2,1,0:T(8,128)(2,1)S(1)}, u32[]{:S(2)}, u32[]{:S(2)}) %all-to-all-start) | async-done | bytes 524320 | tf_op jit(solution)/shard_map/all_to_all | solution.py:15
  32.4 0.2 fusion.48
  32.6 0.2 multiply_reduce_fusion
  33.0 0.2 fusion.24
  33.5 0.1 convert_reduce_fusion.2
  33.6 0.1 multiply_convert_fusion
  33.8 1.5 %fusion.17 = bf16[64,8,1024]{2,1,0:T(8,128)(2,1)} fusion(bf16[64,2048]{1,0:T(8,128)(2,1)S(1)} %multiply_convert_fusion, s32[]{:T(128)S(6)} %select_n.31, bf16[64,512]{1,0:T(8,128)(2,1)S(1)} %convert_reduce_fusion.2), kind=kOutput, calls=%fused_computation.23 | convolution fusion | flops 67633152 | bytes 1245188 | tf_op jit(solution)/shard_map/dot_general | solution.py:144
  35.2 11.2 %all-to-all-start.1 = ((bf16[64,8,1024]{2,1,0:T(8,128)(2,1)}), bf16[64,8,1024]{2,1,0:T(8,128)(2,1)S(1)}, u32[]{:S(2)}, u32[]{:S(2)}) async-start(bf16[64,8,1024]{2,1,0:T(8,128)(2,1)} %fusion.17), calls=%async_computation.1 | async-start | bytes 2097152 | tf_op jit(solution)/shard_map/all_to_all | solution.py:148
  46.5 1.6 %fusion.71 = f32[64,256]{1,0:T(8,128)S(1)} fusion(bf16[64,2048]{1,0:T(8,128)(2,1)} %copy-done.5, bf16[2048,256]{1,0:T(8,128)(2,1)} %param.34), kind=kOutput, calls=%fused_computation.104 | convolution fusion | flops 67108864 | bytes 1376256 | tf_op jit(solution)/shard_map/dot_general | solution.py:164
  48.1 3.1 %convolution_convert_fusion.1 = bf16[64,2048]{1,0:T(8,128)(2,1)} fusion(bf16[256,2048]{1,0:T(8,128)(2,1)} %param.36, bf16[64,2048]{1,0:T(8,128)(2,1)} %copy-done.5, bf16[2048,256]{1,0:T(8,128)(2,1)} %param.35, f32[64,256]{1,0:T(8,128)S(1)} %fusion.71), kind=kOutput, calls=%fused_computation.7 | convolution fusion | flops 134447104 | bytes 2686976 | tf_op jit(solution)/shard_map/dot_general | solution.py:167
  51.2 1.7 %copy.74 = bf16[8,2,8,1024]{3,2,0,1:T(8,128)(2,1)} copy(bf16[8,2,8,1024]{3,2,1,0:T(8,128)(2,1)} %bitcast.85) | data formatting | bytes 524288 | tf_op jit(solution)/shard_map/reshape | solution.py:34
  52.9 11.7 %all-to-all-done.1 = bf16[64,8,1024]{2,1,0:T(8,128)(2,1)S(1)} async-done(((bf16[64,8,1024]{2,1,0:T(8,128)(2,1)}), bf16[64,8,1024]{2,1,0:T(8,128)(2,1)S(1)}, u32[]{:S(2)}, u32[]{:S(2)}) %all-to-all-start.1) | async-done | bytes 1048608 | tf_op jit(solution)/shard_map/all_to_all | solution.py:148
  64.6 1.0 copy-done.4
  65.6 1.5 %copy.61 = bf16[512,1024]{0,1:T(8,128)(2,1)S(1)} copy(bf16[512,1024]{1,0:T(8,128)(2,1)} %bitcast.83) | data formatting | bytes 2097152 | tf_op jit(solution)/shard_map/broadcast_in_dim | solution.py:15
  67.1 0.1 broadcast_in_dim.57
  67.2 7.0 %all_to_all.30 = bf16[2,512,1024]{1,2,0:T(8,128)(2,1)S(1)} all-to-all(bf16[2,512,1024]{1,2,0:T(8,128)(2,1)S(1)} %broadcast_in_dim.57), channel_id=1, replica_groups=mesh['ep'=64,'tp'=2] {'tp'}, dimensions={0} | all-to-all | bytes 4194304 | tf_op jit(solution)/shard_map/all_to_all | solution.py:15
  74.2 1.3 %copy-done.3 = bf16[2,512,1024]{1,2,0:T(8,128)(2,1)} copy-done((bf16[2,512,1024]{1,2,0:T(8,128)(2,1)}, bf16[2,512,1024]{1,2,0:T(8,128)(2,1)S(1)}, u32[]{:S(2)}) %copy-start.3) | copy-done | bytes 2097176
  75.6 0.7 fusion.33
  76.3 5.8 %convolution_convert_fusion = bf16[512,2048]{1,0:T(8,128)(2,1)} fusion(bf16[512,2048]{0,1:T(8,128)(2,1)} %bitcast.81, bf16[1,256,2048]{2,1,0:T(8,128)(2,1)} %param.33, bf16[1,2048,256]{2,1,0:T(8,128)(2,1)} %param.32, f32[512,256]{1,0:T(8,128)S(1)} %fusion.33), kind=kOutput, calls=%fused_computation.6 | convolution fusion | flops 1075576832 | bytes 6815744 | tf_op jit(solution)/shard_map/dot_general | solution.py:155
  82.1 1.8 %copy.73 = bf16[64,2,8,1024]{3,2,0,1:T(8,128)(2,1)S(1)} copy(bf16[64,2,8,1024]{3,2,1,0:T(8,128)(2,1)} %bitcast.84) | data formatting | bytes 4194304 | tf_op jit(solution)/shard_map/reshape | solution.py:34
  83.9 6.3 %all_to_all.31 = bf16[2,512,1024]{2,1,0:T(8,128)(2,1)} all-to-all(bf16[2,512,1024]{2,1,0:T(8,128)(2,1)S(1)} %bitcast.82), channel_id=1, replica_groups=mesh['ep'=64,'tp'=2] {'tp'}, dimensions={0} | all-to-all | bytes 4194304 | tf_op jit(solution)/shard_map/all_to_all | solution.py:40
  90.1 3.8 %all-to-all-start.5 = ((bf16[2,64,1024]{2,1,0:T(8,128)(2,1)}), bf16[2,64,1024]{2,1,0:T(8,128)(2,1)S(1)}, u32[]{:S(2)}, u32[]{:S(2)}) async-start(bf16[2,64,1024]{2,1,0:T(8,128)(2,1)} %bitcast.79), calls=%async_computation.5 | async-start | bytes 524288 | tf_op jit(solution)/shard_map/all_to_all | solution.py:40
  93.9 3.3 %reduce_sum.128 = bf16[512,1024]{1,0:T(8,128)(2,1)} reduce(bf16[2,512,1024]{2,1,0:T(8,128)(2,1)} %all_to_all.31, bf16[]{:T(256)} %constant.43.clone.1), dimensions={0}, to_apply=%region_8.9 | reduce | flops 524288 | bytes 3145730 | tf_op jit(solution)/shard_map/reduce_sum | solution.py:41
  97.3 5.6 %all-to-all-start.4 = ((bf16[64,8,1024]{2,1,0:T(8,128)(2,1)}), bf16[64,8,1024]{2,1,0:T(8,128)(2,1)}, u32[]{:S(2)}, u32[]{:S(2)}) async-start(bf16[64,8,1024]{2,1,0:T(8,128)(2,1)} %bitcast.16), calls=%async_computation.4 | async-start | bytes 2097152 | tf_op jit(solution)/shard_map/all_to_all | solution.py:158
  102.9 1.2 fusion.27
  104.1 0.2 select_reduce_fusion
  104.4 0.8 convolution_convert_fusion.5
  105.2 1.8 %convolution_convert_fusion.6 = bf16[64,64]{1,0:T(8,128)(2,1)} fusion(bf16[64,2048]{1,0:T(8,128)(2,1)S(1)} %copy-done.2, bf16[2048,64]{0,1:T(8,128)(2,1)} %param.24), kind=kOutput, calls=%fused_computation.39 | convolution fusion | flops 16781312 | bytes 532480 | tf_op jit(solution)/shard_map/dot_general | solution.py:100
  107.0 14.2 %all-to-all-done.4 = bf16[64,8,1024]{2,1,0:T(8,128)(2,1)} async-done(((bf16[64,8,1024]{2,1,0:T(8,128)(2,1)}), bf16[64,8,1024]{2,1,0:T(8,128)(2,1)}, u32[]{:S(2)}, u32[]{:S(2)}) %all-to-all-start.4) | async-done | bytes 1048608 | tf_op jit(solution)/shard_map/all_to_all | solution.py:158
  121.3 1.7 %fusion.18 = f32[64,1024]{1,0:T(8,128)S(1)} fusion(bf16[64,8,1024]{2,1,0:T(8,128)(2,1)} %all-to-all-done.4, f32[64,4]{0,1:T(4,128)S(1)} %multiply_divide_fusion, s32[64,4]{0,1:T(4,128)S(1)} %multiply_add_fusion.2), kind=kOutput, calls=%fused_computation.25 | convolution fusion | flops 269287424 | bytes 1312768 | tf_op jit(solution)/shard_map/dot_general | solution.py:159
  123.0 0.2 fusion.68
  123.2 3.5 %all-reduce = (f32[64]{0:T(128)S(1)}, f32[64]{0:T(128)S(1)}) all-reduce(f32[64]{0:T(128)S(1)} %get-tuple-element.4, f32[64]{0:T(128)S(1)} %get-tuple-element.3), channel_id=1, replica_groups=mesh['ep'=64,'tp'=2] {'tp'}, use_global_device_ids=true, to_apply=%region_14.15 | all-reduce | flops 128 | bytes 1024 | tf_op jit(solution)/shard_map/psum | solution.py:171
  126.7 0.8 multiply_convert_fusion.1
  (39 shorter events, 0.7 us)
Async XLA Ops:
  0.6 24.0 %copy-start = (bf16[512,2048]{1,0:T(8,128)(2,1)S(1)}, bf16[512,2048]{1,0:T(8,128)(2,1)}, u32[]{:S(2)}) copy-start(bf16[512,2048]{1,0:T(8,128)(2,1)} %param.27) | copy-start | bytes 6291460
  0.6 2.4 %copy-start.12 = (s32[64]{0:T(128)S(1)}, s32[64]{0:T(128)}, u32[]{:S(2)}) copy-start(s32[64]{0:T(128)} %param.22) | copy-start | bytes 772
  3.2 6.0 %copy-start.13 = (f32[8]{0:T(128)S(1)}, f32[8]{0:T(128)}, u32[]{:S(2)}) copy-start(f32[8]{0:T(128)} %param.26) | copy-start | bytes 100
  7.8 1.4 %copy-start.1 = (f32[64,8,1024]{2,1,0:T(8,128)}, f32[64,8,1024]{2,1,0:T(8,128)S(1)}, u32[]{:S(2)}) copy-start(f32[64,8,1024]{2,1,0:T(8,128)S(1)} %fusion.2) | copy-start | bytes 6291460
  24.6 7.8 %copy-start.2 = (bf16[64,2048]{1,0:T(8,128)(2,1)S(1)}, bf16[64,2048]{1,0:T(8,128)(2,1)}, u32[]{:S(2)}) copy-start(bf16[64,2048]{1,0:T(8,128)(2,1)} %param.19) | copy-start | bytes 786436
  25.1 7.7 %copy-start.9 = (s32[64,4]{0,1:T(4,128)S(1)}, s32[64,4]{0,1:T(4,128)}, u32[]{:S(2)}) copy-start(s32[64,4]{0,1:T(4,128)} %param.30) | copy-start | bytes 3076
  26.0 7.6 %copy-start.10 = (f32[2048]{0:T(1024)S(1)}, f32[2048]{0:T(1024)}, u32[]{:S(2)}) copy-start(f32[2048]{0:T(1024)} %param.28) | copy-start | bytes 24580
  26.0 6.4 %all-to-all-start = ((bf16[2,64,2048]{2,1,0:T(8,128)(2,1)}), bf16[2,64,2048]{2,1,0:T(8,128)(2,1)S(1)}, u32[]{:S(2)}, u32[]{:S(2)}) async-start(bf16[2,64,2048]{2,1,0:T(8,128)(2,1)} %broadcast_in_dim.33), calls=%async_computation | async-start | bytes 1048576 | tf_op jit(solution)/shard_map/all_to_all | solution.py:15
  33.8 1.5 %copy-start.5 = (bf16[64,2048]{1,0:T(8,128)(2,1)}, bf16[64,2048]{1,0:T(8,128)(2,1)S(1)}, u32[]{:S(2)}) copy-start(bf16[64,2048]{1,0:T(8,128)(2,1)S(1)} %multiply_convert_fusion) | copy-start | bytes 786436
  35.2 29.3 %all-to-all-start.1 = ((bf16[64,8,1024]{2,1,0:T(8,128)(2,1)}), bf16[64,8,1024]{2,1,0:T(8,128)(2,1)S(1)}, u32[]{:S(2)}, u32[]{:S(2)}) async-start(bf16[64,8,1024]{2,1,0:T(8,128)(2,1)} %fusion.17), calls=%async_computation.1 | async-start | bytes 2097152 | tf_op jit(solution)/shard_map/all_to_all | solution.py:148
  64.6 1.0 copy-start.4
  67.2 8.4 %copy-start.7 = (bf16[1,2048,256]{2,1,0:T(8,128)(2,1)S(1)}, bf16[1,2048,256]{2,1,0:T(8,128)(2,1)}, u32[]{:S(2)}) copy-start(bf16[1,2048,256]{2,1,0:T(8,128)(2,1)} %param.31) | copy-start | bytes 3145732
  74.2 1.4 %copy-start.3 = (bf16[2,512,1024]{1,2,0:T(8,128)(2,1)}, bf16[2,512,1024]{1,2,0:T(8,128)(2,1)S(1)}, u32[]{:S(2)}) copy-start(bf16[2,512,1024]{1,2,0:T(8,128)(2,1)S(1)} %all_to_all.30) | copy-start | bytes 6291460
  90.1 7.1 %all-to-all-start.5 = ((bf16[2,64,1024]{2,1,0:T(8,128)(2,1)}), bf16[2,64,1024]{2,1,0:T(8,128)(2,1)S(1)}, u32[]{:S(2)}, u32[]{:S(2)}) async-start(bf16[2,64,1024]{2,1,0:T(8,128)(2,1)} %bitcast.79), calls=%async_computation.5 | async-start | bytes 524288 | tf_op jit(solution)/shard_map/all_to_all | solution.py:40
  93.9 9.0 %copy-start.6 = (bf16[64,2048]{1,0:T(8,128)(2,1)S(1)}, bf16[64,2048]{1,0:T(8,128)(2,1)}, u32[]{:S(2)}) copy-start(bf16[64,2048]{1,0:T(8,128)(2,1)} %copy-done.5) | copy-start | bytes 786436
  97.3 7.1 %copy-start.8 = (bf16[2048,64]{0,1:T(8,128)(2,1)S(1)}, bf16[2048,64]{0,1:T(8,128)(2,1)}, u32[]{:S(2)}) copy-start(bf16[2048,64]{0,1:T(8,128)(2,1)} %param.25) | copy-start | bytes 786436
  97.3 24.0 %all-to-all-start.4 = ((bf16[64,8,1024]{2,1,0:T(8,128)(2,1)}), bf16[64,8,1024]{2,1,0:T(8,128)(2,1)}, u32[]{:S(2)}, u32[]{:S(2)}) async-start(bf16[64,8,1024]{2,1,0:T(8,128)(2,1)} %bitcast.16), calls=%async_computation.4 | async-start | bytes 2097152 | tf_op jit(solution)/shard_map/all_to_all | solution.py:158
  104.4 22.3 %copy-start.11 = (f32[1024]{0:T(1024)S(1)}, f32[1024]{0:T(1024)}, u32[]{:S(2)}) copy-start(f32[1024]{0:T(1024)} %param.37) | copy-start | bytes 12292
where the time goes:
time: 128 us; the launch traced here: 127 us
  matrix products  35.6 us (28%)
  waiting for transfers between devices  27.3 us (21%)
  starting transfers between devices  25.7 us (20%)
  blocking collectives  16.7 us (13%)
  local copies, waits for them, and re-layouts  14 us (11%)
  other arithmetic  7.26 us (6%)
    all_to_all x1, waiting for transfers between devices, on_device(): lax.all_to_all(back_rows, 'ep', split_axis=0, concat_axis=0, tiled=True)  14.2 us
    all_to_all x1, waiting for transfers between devices, on_device(): lax.all_to_all(outgoing, 'ep', split_axis=0, concat_axis=0, tiled=True)  11.7 us
    all_to_all x1, starting transfers between devices, on_device(): lax.all_to_all(outgoing, 'ep', split_axis=0, concat_axis=0, tiled=True)  11.2 us
    dot_general x1, matrix products, on_device(): jnp.einsum('skgc,skdc->skgd', stick_weight, cache_values, preferred_eleme...  7 us
    all_to_all x1, blocking collectives, sent_to_all(): lax.all_to_all(jnp.broadcast_to(x[None], (length, *x.shape)), axis, 0, 0,...  6.99 us
    all_to_all x1, blocking collectives, summed_on_arrival(): lax.all_to_all(tiles, axis, split_axis=0, concat_axis=0, tiled=True)  6.26 us
    dot_general x1, matrix products, on_device(): jnp.dot(inner, expert_down[0], preferred_element_type=jnp.float32)  5.8 us
    all_to_all x1, starting transfers between devices, on_device(): lax.all_to_all(back_rows, 'ep', split_axis=0, concat_axis=0, tiled=True)  5.64 us
  transfers between devices with their start and end apart: 4, of which 3 were waited for; matrix products, arithmetic and copies ran while one was open for 11% of the time, Pallas kernels for 0%

commit v1 on v0

v1 whole, which is shorter than its diff:
```python
import functools

import jax
import jax.numpy as jnp
from jax import lax
from jax.experimental import pallas as pl
from jax.experimental.pallas import tpu as pltpu
from jax.sharding import PartitionSpec as P

RESIDUAL_SCALE = 2.0**0.25
ROUTE_SCALE = 2.5
NORM_EPS = 1e-05
F32 = jnp.float32
BF16 = jnp.bfloat16
VMEM = pltpu.VMEM
SEQ_STEP = 8
CUM = 256
AHEAD = 3


def iota(shape, dim):
    return lax.broadcasted_iota(jnp.int32, shape, dim)


def dot(a, b):
    return jnp.dot(a, b, preferred_element_type=F32)


def dot_nt(a, b):
    return lax.dot_general(a, b, (((1,), (1,)), ((), ())), preferred_element_type=F32)


def whole():
    return pl.BlockSpec(memory_space=VMEM)


def in_hbm(*arrays):
    return [pltpu.with_memory_space_constraint(x, pltpu.HBM) for x in arrays]


def swapped(x):
    return lax.ppermute(x, "tp", [(0, 1), (1, 0)])


def attend_kernel(
    len_hbm, bias_hbm, x_hbm, wq_hbm, k_hbm, v_hbm, wo_hbm, o_ref,
    len_scr, bias_scr, x_scr, wq_scr, k_scr, v_scr, wo_scr, q_scr, at_scr, tri_scr,
    sems, k_sems, v_sems,
):
    seqs, size, length = k_scr.shape
    heads = bias_scr.shape[0]
    blocks = length // CUM
    steps = seqs // SEQ_STEP
    small = [
        pltpu.make_async_copy(src, dst, sems.at[i])
        for i, (src, dst) in enumerate(
            [(x_hbm, x_scr), (wq_hbm, wq_scr), (len_hbm, len_scr), (bias_hbm, bias_scr)]
        )
    ]
    wo_copy = pltpu.make_async_copy(wo_hbm, wo_scr, sems.at[4])

    def cache_copies(step):
        part = pl.ds(step * SEQ_STEP, SEQ_STEP)
        return (
            pltpu.make_async_copy(k_hbm.at[part], k_scr.at[part], k_sems.at[step]),
            pltpu.make_async_copy(v_hbm.at[part], v_scr.at[part], v_sems.at[step]),
        )

    for copy in small:
        copy.start()
    for step in range(AHEAD):
        for copy in cache_copies(step):
            copy.start()
    row, col = iota((CUM, CUM), 0), iota((CUM, CUM), 1)
    tri_scr[...] = jnp.where(row > col, 1.0, 0.0).astype(BF16)
    for copy in small:
        copy.wait()
    query = dot(x_scr[...], wq_scr[...]).astype(BF16).astype(F32) * size**-0.5
    for g in range(heads):
        q_scr[pl.ds(g, seqs, stride=heads), :] = query[:, g * size : (g + 1) * size]
    head = iota((heads, 1), 0)
    bias = jnp.zeros((heads, 1), F32)
    for g in range(heads):
        bias = jnp.where(head == g, bias_scr[g], bias)
    position = iota((heads, length), 1)

    def one_step(step, carry):
        k_copy, v_copy = cache_copies(step)

        @pl.when(step + AHEAD < steps)
        def _():
            for copy in cache_copies(step + AHEAD):
                copy.start()

        @pl.when(step + AHEAD == steps)
        def _():
            wo_copy.start()

        k_copy.wait()
        scores, usable, soft = [], [], []
        for i in range(SEQ_STEP):
            seq = step * SEQ_STEP + i
            query = q_scr[pl.ds(pl.multiple_of(seq * heads, heads), heads), :]
            x = dot(query.astype(BF16), k_scr[seq]) + bias
            ok = position < len_scr[seq]
            sp = jnp.maximum(x, 0.0) + jnp.log(1.0 + jnp.exp(-jnp.abs(x)))
            scores.append(x - sp)
            usable.append(ok)
            soft.append(jnp.where(ok, sp, 0.0).astype(BF16))
        stacked = jnp.concatenate(
            [s[:, b * CUM : (b + 1) * CUM] for s in soft for b in range(blocks)], axis=0
        )
        sums = dot(stacked, tri_scr[...])
        totals = sums[:, :1] + stacked[:, :1].astype(F32)
        v_copy.wait()
        for i in range(SEQ_STEP):
            base = i * blocks * heads
            after = jnp.zeros((heads, 1), F32)
            parts = [None] * blocks
            for b in reversed(range(blocks)):
                rows = slice(base + b * heads, base + (b + 1) * heads)
                parts[b] = sums[rows, :] + after
                after = after + totals[rows]
            later = jnp.concatenate(parts, axis=1)
            weight = jnp.where(usable[i], jnp.exp(scores[i] - later), 0.0).astype(BF16)
            seq = step * SEQ_STEP + i
            at_scr[pl.ds(pl.multiple_of(seq * heads, heads), heads), :] = dot_nt(weight, v_scr[seq])
        return carry

    lax.fori_loop(0, steps, one_step, 0)
    attended = jnp.concatenate(
        [at_scr[pl.ds(g, seqs, stride=heads), :] for g in range(heads)], axis=1
    ).astype(BF16)
    wo_copy.wait()
    o_ref[...] = dot(attended, wo_scr[...]).astype(BF16)


def attend(inputs, keys, values, lengths, wq, head_bias, wo):
    seqs, width = inputs.shape
    size, length = keys.shape[1:]
    heads = head_bias.shape[0]
    steps = seqs // SEQ_STEP
    return pl.pallas_call(
        attend_kernel,
        out_shape=jax.ShapeDtypeStruct((seqs, width), BF16),
        in_specs=[pl.BlockSpec(memory_space=pl.ANY)] * 7,
        out_specs=whole(),
        scratch_shapes=[
            pltpu.SMEM((seqs,), jnp.int32),
            pltpu.SMEM((heads,), F32),
            VMEM(inputs.shape, BF16),
            VMEM(wq.shape, BF16),
            VMEM(keys.shape, BF16),
            VMEM(values.shape, BF16),
            VMEM(wo.shape, BF16),
            VMEM((seqs * heads, size), F32),
            VMEM((seqs * heads, size), F32),
            VMEM((CUM, CUM), BF16),
            pltpu.SemaphoreType.DMA((5,)),
            pltpu.SemaphoreType.DMA((steps,)),
            pltpu.SemaphoreType.DMA((steps,)),
        ],
        compiler_params=pltpu.CompilerParams(vmem_limit_bytes=36 * 2**20),
        cost_estimate=pl.CostEstimate(
            flops=8 * 10**9, bytes_accessed=22 * 10**6, transcendentals=2 * 10**6
        ),
        name="attend",
    )(*in_hbm(lengths, head_bias, inputs, wq, keys, values, wo))


def place_kernel(core_ref, routes_ref, place_ref, member_ref):
    choices, lanes = routes_ref.shape
    experts = member_ref.shape[0]
    rows = place_ref.shape[0]
    half = lanes // 2
    slots = rows // experts // 2
    expert = iota((experts, lanes), 0)
    named = expert == routes_ref[0:1, :]
    for k in range(1, choices):
        named = named | (expert == routes_ref[k : k + 1, :])
    member = jnp.where(named, 1.0, 0.0)
    member_ref[...] = member
    a, b = iota((lanes, lanes), 0), iota((lanes, lanes), 1)
    earlier = jnp.where((a < b) & ((a < half) == (b < half)), 1.0, 0.0).astype(BF16)
    slot = dot(member.astype(BF16), earlier)
    code = ((slot + 1.0) * member).astype(BF16)
    r, e = iota((rows, experts), 0), iota((rows, experts), 1)
    spread = jnp.where(r // (2 * slots) == e, 1.0, 0.0).astype(BF16)
    found = dot(spread, code)
    r, lane = iota((rows, lanes), 0), iota((rows, lanes), 1)
    wanted = (r % slots + 1 + core_ref[0] * slots).astype(F32)
    same_half = ((r // slots) % 2 == 0) == (lane < half)
    place_ref[...] = jnp.where((found == wanted) & same_half, 1.0, 0.0).astype(BF16)


def place(core, routes2, experts, slots):
    lanes = routes2.shape[1]
    return pl.pallas_call(
        place_kernel,
        out_shape=(
            jax.ShapeDtypeStruct((experts * 2 * slots, lanes), BF16),
            jax.ShapeDtypeStruct((experts, lanes), F32),
        ),
        in_specs=[pl.BlockSpec(memory_space=pltpu.SMEM), whole()],
        out_specs=(whole(), whole()),
        compiler_params=pltpu.CompilerParams(vmem_limit_bytes=8 * 2**20),
        cost_estimate=pl.CostEstimate(flops=10**8, bytes_accessed=10**5, transcendentals=0),
        name="place",
    )(core, routes2)


def halves(x):
    half = x.shape[1] // 2
    return jnp.concatenate([x[:, :half], x[:, half:]], axis=0)


def dispatch_kernel(
    x_ref, own_ref, other_ref, gain_ref, place_ref, hidden_hbm, out_ref, hidden_scr, sem
):
    v = (
        RESIDUAL_SCALE * x_ref[...].astype(F32)
        + own_ref[...].astype(F32)
        + other_ref[...].astype(F32)
    )
    centered = v - jnp.mean(v, axis=1, keepdims=True)
    var = jnp.mean(centered * centered, axis=1, keepdims=True)
    hidden = (centered * lax.rsqrt(var + NORM_EPS) * gain_ref[...]).astype(BF16)
    hidden_scr[...] = hidden
    copy = pltpu.make_async_copy(hidden_scr, hidden_hbm, sem)
    copy.start()
    out_ref[...] = dot(place_ref[...], halves(hidden)).astype(BF16)
    copy.wait()


def dispatch(inputs, own, other, gain, placement):
    seqs, width = inputs.shape
    return pl.pallas_call(
        dispatch_kernel,
        out_shape=(
            pltpu.HBM((seqs, width), BF16),
            jax.ShapeDtypeStruct((placement.shape[0], width // 2), BF16),
        ),
        in_specs=[whole()] * 5,
        out_specs=(pl.BlockSpec(memory_space=pltpu.HBM), whole()),
        scratch_shapes=[VMEM((seqs, width), BF16), pltpu.SemaphoreType.DMA],
        compiler_params=pltpu.CompilerParams(vmem_limit_bytes=12 * 2**20),
        cost_estimate=pl.CostEstimate(flops=2 * 10**8, bytes_accessed=2 * 10**6, transcendentals=64),
        name="dispatch",
    )(inputs, own, other, gain.reshape(1, width), placement)


def local_kernel(
    hidden_ref, x_ref, router_ref, member_ref, place_ref, sg_ref, su_ref, sd_ref, wk_ref, wv_ref,
    shared_ref, weight_ref, nk_ref, nv_ref,
):
    hidden = hidden_ref[...]
    gate, up = dot(hidden, sg_ref[...]), dot(hidden, su_ref[...])
    inner = (gate / (1.0 + jnp.exp(-gate)) * up).astype(BF16)
    shared_ref[...] = dot(inner, sd_ref[...])
    probs = 1.0 / (1.0 + jnp.exp(-dot_nt(router_ref[...], hidden)))
    probs = jnp.concatenate([probs, probs], axis=1) * member_ref[...]
    weights = ROUTE_SCALE * probs / jnp.sum(probs, axis=0, keepdims=True)
    experts = weights.shape[0]
    rows, lanes = place_ref.shape
    r, e = iota((rows, experts), 0), iota((rows, experts), 1)
    spread = jnp.where(r // (rows // experts) == e, 1.0, 0.0)
    placed = jnp.dot(spread, weights, precision=lax.Precision.HIGHEST, preferred_element_type=F32)
    placed = (placed * place_ref[...].astype(F32)).T
    high = placed.astype(BF16)
    weight_ref[:lanes, :] = high
    weight_ref[lanes:, :] = (placed - high.astype(F32)).astype(BF16)
    x = x_ref[...]
    nk_ref[...] = dot_nt(x, wk_ref[...]).astype(BF16)
    nv_ref[...] = dot_nt(x, wv_ref[...]).astype(BF16)


def local(hidden, inputs, router_t, member, placement, sg, su, sd, wk_t, wv_t):
    seqs, width = hidden.shape
    rows, lanes = placement.shape
    size = wk_t.shape[0]
    return pl.pallas_call(
        local_kernel,
        out_shape=(
            jax.ShapeDtypeStruct((seqs, width), F32),
            jax.ShapeDtypeStruct((2 * lanes, rows), BF16),
            jax.ShapeDtypeStruct((seqs, size), BF16),
            jax.ShapeDtypeStruct((seqs, size), BF16),
        ),
        in_specs=[whole()] * 10,
        out_specs=(whole(),) * 4,
        compiler_params=pltpu.CompilerParams(vmem_limit_bytes=20 * 2**20),
        cost_estimate=pl.CostEstimate(
            flops=4 * 10**9, bytes_accessed=5 * 10**6, transcendentals=10**5
        ),
        name="local",
    )(hidden, inputs, router_t, member, placement, *in_hbm(sg, su, sd, wk_t, wv_t))


def expert_kernel(order_ref, rows_ref, *refs):
    weights, out_ref = refs[:-1], refs[-1]
    groups, lines, half = rows_ref.shape
    slots = lines // 2
    low = iota((groups // 2, lines, half), 1) < slots
    x = rows_ref[...].astype(F32).reshape(groups // 2, 2, lines, half)
    a, b = x[:, 0], x[:, 1]
    count = groups * slots
    first = jnp.where(low, a, pltpu.roll(b, slots, 1)).reshape(count, half).astype(BF16)
    second = jnp.where(low, pltpu.roll(a, slots, 1), b).reshape(count, half).astype(BF16)
    total = None
    for i in range(2):
        gate_ref, up_ref, down_ref = weights[3 * i : 3 * i + 3]
        gate = dot(first, gate_ref[:half, :]) + dot(second, gate_ref[half:, :])
        up = dot(first, up_ref[:half, :]) + dot(second, up_ref[half:, :])
        inner = (gate / (1.0 + jnp.exp(-gate)) * up).astype(BF16)
        part = dot(inner, down_ref[...]).astype(BF16).astype(F32)
        total = part if total is None else total + part
    a = total[:, :half].reshape(groups // 2, lines, half)
    b = total[:, half:].reshape(groups // 2, lines, half)
    even = jnp.where(low, a, pltpu.roll(b, slots, 1))
    odd = jnp.where(low, pltpu.roll(a, slots, 1), b)
    out_ref[...] = jnp.stack([even, odd], axis=1).reshape(groups, lines, half).astype(BF16)


def expert(order, rows, weights):
    return pl.pallas_call(
        expert_kernel,
        out_shape=jax.ShapeDtypeStruct(rows.shape, BF16),
        in_specs=[pl.BlockSpec(memory_space=pl.ANY)] + [whole()] * 7,
        out_specs=whole(),
        compiler_params=pltpu.CompilerParams(vmem_limit_bytes=32 * 2**20),
        cost_estimate=pl.CostEstimate(
            flops=2 * 10**9, bytes_accessed=8 * 10**6, transcendentals=3 * 10**5
        ),
        name="expert",
    )(*in_hbm(order), rows, *weights)


def combine_kernel(weight_ref, rows_ref, shared_ref, mine_ref, send_ref):
    lanes = weight_ref.shape[0] // 2
    both = dot(weight_ref[...], rows_ref[...])
    part = both[:lanes, :] + both[lanes:, :] + halves(shared_ref[...])
    mine_ref[...] = part
    send_ref[...] = part.astype(BF16)


def combine(weight, rows, shared):
    shape = (weight.shape[0] // 2, rows.shape[1])
    return pl.pallas_call(
        combine_kernel,
        out_shape=(jax.ShapeDtypeStruct(shape, F32), jax.ShapeDtypeStruct(shape, BF16)),
        in_specs=[whole()] * 3,
        out_specs=(whole(), whole()),
        compiler_params=pltpu.CompilerParams(vmem_limit_bytes=16 * 2**20),
        cost_estimate=pl.CostEstimate(flops=3 * 10**8, bytes_accessed=3 * 10**6, transcendentals=0),
        name="combine",
    )(weight, rows, shared)


def finish_kernel(core_ref, mine_ref, other_ref, hidden_ref, gain_ref, out_ref, mixed):
    seqs, half = out_ref.shape
    v = mine_ref[...] + other_ref[...].astype(F32) + RESIDUAL_SCALE * halves(hidden_ref[...]).astype(F32)
    mixed[...] = v
    sums = jnp.sum(v, axis=1, keepdims=True)
    mean = (sums[:seqs] + sums[seqs:]) / (2 * half)
    centered = v - jnp.concatenate([mean, mean], axis=0)
    squares = jnp.sum(centered * centered, axis=1, keepdims=True)
    scale = lax.rsqrt((squares[:seqs] + squares[seqs:]) / (2 * half) + NORM_EPS)
    own = mixed[pl.ds(pl.multiple_of(core_ref[0] * seqs, seqs), seqs), :]
    out_ref[...] = ((own - mean) * scale * gain_ref[...]).astype(BF16)


def finish(core, mine, other, hidden, gain):
    lanes, half = mine.shape
    return pl.pallas_call(
        finish_kernel,
        out_shape=jax.ShapeDtypeStruct((lanes // 2, half), BF16),
        in_specs=[pl.BlockSpec(memory_space=pltpu.SMEM)] + [whole()] * 4,
        out_specs=whole(),
        scratch_shapes=[VMEM((lanes, half), F32)],
        compiler_params=pltpu.CompilerParams(vmem_limit_bytes=12 * 2**20),
        cost_estimate=pl.CostEstimate(flops=10**7, bytes_accessed=2 * 10**6, transcendentals=64),
        name="finish",
    )(core, mine, other, hidden, gain.reshape(1, half))


def on_device(
    inputs,
    cache_keys,
    cache_values,
    lengths,
    query_weight,
    key_weight,
    value_weight,
    head_bias,
    out_weight,
    attend_gain,
    router_weight,
    routes,
    expert_gate,
    expert_up,
    expert_down,
    shared_gate,
    shared_up,
    shared_down,
    final_gain,
):
    seqs, width = inputs.shape
    experts = router_weight.shape[1]
    slots = 2 * seqs * routes.shape[1] // experts // 2
    core = lax.axis_index("tp").astype(jnp.int32).reshape(1)
    own_part = attend(
        inputs, cache_keys[:, 0], cache_values[:, 0], lengths, query_weight, head_bias, out_weight
    )
    other_part = swapped(own_part)
    routes_t = routes.T
    placement, member = place(core, jnp.concatenate([routes_t, routes_t], axis=1), experts, slots)
    hidden, outgoing = dispatch(inputs, own_part, other_part, attend_gain, placement)
    arrived = lax.all_to_all(
        outgoing.reshape(experts, 2 * slots, width // 2), "ep", 0, 0, tiled=True
    )
    own_weights = (expert_gate[0], expert_up[0], expert_down[0])
    other_weights = tuple(swapped(w) for w in own_weights)
    shared, weight, new_keys, new_values = local(
        hidden, inputs, router_weight.T, member, placement, shared_gate, shared_up, shared_down,
        key_weight.T, value_weight.T,
    )
    results = expert(new_keys, arrived, own_weights + other_weights)
    returned = lax.all_to_all(results, "ep", 0, 0, tiled=True)
    mine, send = combine(weight, returned.reshape(experts * 2 * slots, width // 2), shared)
    output = finish(core, mine, swapped(send), hidden, final_gain)
    return (output, new_keys, new_values)


def solution(mesh):
    placed = (
        P("ep", None),
        P("ep", "tp", None, None),
        P("ep", "tp", None, None),
        P("ep"),
        P(None, "tp"),
        P(None, "tp"),
        P(None, "tp"),
        P("tp"),
        P("tp", None),
        P(),
        P(),
        P("ep", None),
        P("ep", None, "tp"),
        P("ep", None, "tp"),
        P("ep", "tp", None),
        P(None, "tp"),
        P(None, "tp"),
        P("tp", None),
        P("tp"),
    )
    return jax.shard_map(
        on_device,
        mesh=mesh,
        in_specs=placed,
        out_specs=(P("ep", "tp"), P("ep", "tp"), P("ep", "tp")),
        check_vma=False,
    )
```

time: 128 us -> 77.2 us (0.60)
  matrix products: 35.6 us -> 0 us
  Pallas kernels: 0 us -> 23.1 us
  waiting for transfers between devices: 27.3 us -> 11.1 us
  local copies, waits for them, and re-layouts: 14 us -> 4.21 us
  starting transfers between devices: 25.7 us -> 16.6 us
  other arithmetic: 7.26 us -> 0.07 us
  blocking collectives: 16.7 us -> 21 us
    dot_general x16 -> x0, matrix products: 35.6 us -> none  [the longest x1 7 us: on_device(): jnp.einsum('skgc,skdc->skgd', stick_weight, cache_values, preferred_eleme...]
    pallas_call x0 -> x7, Pallas kernels: none -> 23.1 us  [the longest x1 10.5 us: attend(): pl.pallas_call(attend_kernel, out_shape=jax.ShapeDtypeStruct((seqs, width...]
    all_to_all x4 -> x1, waiting for transfers between devices: 27.3 us -> 9.85 us  [on_device(): lax.all_to_all(outgoing.reshape(experts, 2 * slots, width // 2), 'ep', 0,...]
    all_to_all x4 -> x1, starting transfers between devices: 25.7 us -> 11.3 us  [on_device(): lax.all_to_all(outgoing.reshape(experts, 2 * slots, width // 2), 'ep', 0,...]
    all_to_all x2 -> x1, blocking collectives: 13.2 us -> 21 us  [on_device(): returned = lax.all_to_all(results, 'ep', 0, 0, tiled=True)]
    reshape x4 -> x0, local copies, waits for them, and re-layouts: 6.29 us -> none  [the longest x2 3.43 us: cut_along(): tiles = x.reshape(*dims[:dim], length, dims[dim] // length, *dims[dim + 1:])]
    reduce_sum x9 -> x0, other arithmetic: 6.21 us -> none  [the longest x2 3.37 us: summed_on_arrival(): return arrived.astype(jnp.float32).sum(axis=0)]
    ppermute x0 -> x5, starting transfers between devices: none -> 5.31 us  [swapped(): return lax.ppermute(x, 'tp', [(0, 1), (1, 0)])]
  transfers between devices with their start and end apart: 4 -> 6, of which waited for: 3 -> 3; matrix products, arithmetic and copies ran while one was open for 11% -> 0% of each run, Pallas kernels for 0% -> 9%
where the time goes in v1:
time: 77.2 us; the launch traced here: 76.8 us
  Pallas kernels  23.1 us (30%)
  blocking collectives  21 us (27%)
  starting transfers between devices  16.6 us (22%)
  waiting for transfers between devices  11.1 us (14%)
  local copies, waits for them, and re-layouts  4.21 us (5%)
    all_to_all x1, blocking collectives, on_device(): returned = lax.all_to_all(results, 'ep', 0, 0, tiled=True)  21 us
    all_to_all x1, starting transfers between devices, on_device(): lax.all_to_all(outgoing.reshape(experts, 2 * slots, width // 2), 'ep', 0,...  11.3 us
    pallas_call x1, Pallas kernels, attend(): pl.pallas_call(attend_kernel, out_shape=jax.ShapeDtypeStruct((seqs, width...  10.5 us
    all_to_all x1, waiting for transfers between devices, on_device(): lax.all_to_all(outgoing.reshape(experts, 2 * slots, width // 2), 'ep', 0,...  9.85 us
    ppermute x5, starting transfers between devices, swapped(): return lax.ppermute(x, 'tp', [(0, 1), (1, 0)])  5.31 us
    pallas_call x1, Pallas kernels, expert(): pl.pallas_call(expert_kernel, out_shape=jax.ShapeDtypeStruct(rows.shape,...  4.47 us
    unnamed x30, local copies, waits for them, and re-layouts  4.21 us
    pallas_call x1, Pallas kernels, local(): pl.pallas_call(local_kernel, out_shape=(jax.ShapeDtypeStruct((seqs, width...  4.03 us
  transfers between devices with their start and end apart: 6, of which 3 were waited for; matrix products, arithmetic and copies ran while one was open for 0% of the time, Pallas kernels for 9%

profile of v1, /device:TPU:1, one launch (start us, length us, event | category | flops | bytes accessed | tf_op | source)
XLA Modules:
  0.0 76.8 jit_solution(10607962806348685401)
XLA Ops:
  0.6 0.0 copy-start
  0.6 0.0 copy-start.1
  0.7 0.0 copy-start.14
  0.7 0.0 copy-start.4
  0.7 0.0 copy-start.9
  0.7 10.5 %attend.1.own_ref = bf16[64,2048]{1,0:T(8,128)(2,1)S(1)} custom-call(s32[64]{0:T(128)} %len_hbm.1, f32[8]{0:T(128)} %bias_hbm.1, bf16[64,2048]{1,0:T(8,128)(2,1)} %x_ref.3, bf16[2048,512]{1,0:T(8,128)(2,1)} %wq_hbm.1, bf16[64,64,1024]{2,1,0:T(8,128)(2,1)} %bitcast.23, bf16[64,64,1024]{2,1,0:T(8,128)(2,1)} %bitcast.24, bf16[512,2048]{1,0:T(8,128)(2,1)} %wo_hbm.1), custom_call_target="tpu_custom_call" | custom-call | flops 8000000000 | bytes 22000000 | tf_op jit(solution)/shard_map/attend/pallas_call | solution.py:143
  11.2 1.5 %collective-permute-start = (bf16[64,2048]{1,0:T(8,128)(2,1)S(1)}, bf16[64,2048]{1,0:T(8,128)(2,1)S(1)}, u32[]{:S(2)}, u32[]{:S(2)}) collective-permute-start(bf16[64,2048]{1,0:T(8,128)(2,1)S(1)} %attend.1.own_ref), channel_id=1, source_target_pairs={{0,1},{1,0},{2,3},{3,2},{4,5},{5,4},{6,7},{7,6},{8,9},{9,8},{10,11... | collective-permute-start | bytes 786440 | tf_op jit(solution)/shard_map/ppermute | solution.py:42
  12.7 0.0 copy-done
  12.7 0.1 collective-permute-start.1
  12.8 0.0 copy-done.1
  12.8 0.4 collective-permute-start.2
  13.2 0.1 collective-permute-start.3
  13.3 0.0 copy-done.14
  13.3 0.1 pad_add_fusion.routes_ref
  13.3 0.3 place.1
  13.7 0.0 copy-start.12
  13.7 0.1 collective-permute-done.other_ref
  13.8 0.0 copy-done.4
  13.8 0.0 copy-done.9
  13.8 2.2 %dispatch.1 = (bf16[64,2048]{1,0:T(8,128)(2,1)}, bf16[512,1024]{1,0:T(8,128)(2,1)}) custom-call(bf16[64,2048]{1,0:T(8,128)(2,1)S(1)} %copy-done.4, bf16[64,2048]{1,0:T(8,128)(2,1)S(1)} %attend.1.own_ref, bf16[64,2048]{1,0:T(8,128)(2,1)S(1)} %collective-permute-done.other_ref, f32[1,2048]{1,0:T(1,128)S(1)} %bitcast.19, ...), custom_call_target="tpu_custom_call" | custom-call | flops 200000000 | bytes 2000000 | tf_op jit(solution)/shard_map/dispatch/pallas_call | solution.py:237
  16.1 0.0 copy-done.12
  16.1 11.3 %all-to-all-start = ((bf16[64,8,1024]{2,1,0:T(8,128)(2,1)}), bf16[64,8,1024]{2,1,0:T(8,128)(2,1)S(1)}, u32[]{:S(2)}, u32[]{:S(2)}) async-start(bf16[64,8,1024]{2,1,0:T(8,128)(2,1)} %bitcast.8), calls=%async_computation | async-start | bytes 2097152 | tf_op jit(solution)/shard_map/all_to_all | solution.py:418
  27.3 0.0 copy-start.7
  27.4 0.9 %copy-done.7 = bf16[64,2048]{1,0:T(8,128)(2,1)S(1)} copy-done((bf16[64,2048]{1,0:T(8,128)(2,1)S(1)}, bf16[64,2048]{1,0:T(8,128)(2,1)}, u32[]{:S(2)}) %copy-start.7) | copy-done | bytes 262168
  28.3 0.0 copy-start.11
  28.3 0.9 %copy-done.11 = bf16[2048,64]{0,1:T(8,128)(2,1)S(1)} copy-done((bf16[2048,64]{0,1:T(8,128)(2,1)S(1)}, bf16[2048,64]{0,1:T(8,128)(2,1)}, u32[]{:S(2)}) %copy-start.11) | copy-done | bytes 262168
  29.2 0.0 copy-start.13
  29.3 0.8 copy-done.13
  30.0 4.0 %local.1 = (f32[64,2048]{1,0:T(8,128)S(1)}, bf16[256,512]{1,0:T(8,128)(2,1)S(1)}, bf16[64,64]{1,0:T(8,128)(2,1)}, bf16[64,64]{1,0:T(8,128)(2,1)}) custom-call(bf16[64,2048]{1,0:T(8,128)(2,1)S(1)} %copy-done.7, bf16[64,2048]{1,0:T(8,128)(2,1)S(1)} %copy-done.4, bf16[64,2048]{1,0:T(8,128)(2,1)S(1)} %bitcast.21, f32[64,128]{1,0:T(8,128)S(1)} %copy-done.13, ...), custom_call_target="tpu_custom_call" | custom-call | flops 4000000000 | bytes 5000000 | tf_op jit(solution)/shard_map/local/pallas_call | solution.py:281
  34.0 0.0 copy-start.2
  34.0 0.8 %copy-done.2 = f32[64,2048]{1,0:T(8,128)} copy-done((f32[64,2048]{1,0:T(8,128)}, f32[64,2048]{1,0:T(8,128)S(1)}, u32[]{:S(2)}) %copy-start.2) | copy-done | bytes 524312
  34.8 0.0 copy-start.5
  34.8 0.7 copy-done.5
  35.6 0.0 copy-start.10
  35.6 0.0 collective-permute-done.1.refs_3_
  35.6 0.0 collective-permute-done.2.refs_4_
  35.6 0.0 collective-permute-done.3.refs_5_
  35.6 9.9 %all-to-all-done.rows_ref = bf16[64,8,1024]{2,1,0:T(8,128)(2,1)S(1)} async-done(((bf16[64,8,1024]{2,1,0:T(8,128)(2,1)}), bf16[64,8,1024]{2,1,0:T(8,128)(2,1)S(1)}, u32[]{:S(2)}, u32[]{:S(2)}) %all-to-all-start) | async-done | bytes 1048608 | tf_op jit(solution)/shard_map/all_to_all | solution.py:418
  45.4 4.5 %expert.1 = bf16[64,8,1024]{2,1,0:T(8,128)(2,1)S(1)} custom-call(bf16[64,64]{1,0:T(8,128)(2,1)} %get-tuple-element.11.order_ref, bf16[64,8,1024]{2,1,0:T(8,128)(2,1)S(1)} %all-to-all-done.rows_ref, bf16[2048,256]{1,0:T(8,128)(2,1)S(1)} %bitcast.16, bf16[2048,256]{1,0:T(8,128)(2,1)S(1)} %bitcast.18, bf16[256,2048]{1,0:T(8,128)(2,1)} %bitcast.11.refs_2_, ...), custom_call_target="tpu_custom_call" | custom-call | flops 2000000000 | bytes 8000000 | tf_op jit(solution)/shard_map/expert/pallas_call | solution.py:325
  49.9 21.0 %all_to_all.10 = bf16[64,8,1024]{2,1,0:T(8,128)(2,1)S(1)} all-to-all(bf16[64,8,1024]{2,1,0:T(8,128)(2,1)S(1)} %expert.1), channel_id=1, replica_groups=mesh['ep'=64,'tp'=2] {'ep'}, dimensions={0} | all-to-all | bytes 2097152 | tf_op jit(solution)/shard_map/all_to_all | solution.py:428
  70.9 0.0 copy-done.6
  70.9 0.0 copy-done.3
  70.9 0.4 combine.1
  71.3 3.2 %collective-permute-start.4 = (bf16[128,1024]{1,0:T(8,128)(2,1)S(1)}, bf16[128,1024]{1,0:T(8,128)(2,1)S(1)}, u32[]{:S(2)}, u32[]{:S(2)}) collective-permute-start(bf16[128,1024]{1,0:T(8,128)(2,1)S(1)} %get-tuple-element.21), channel_id=1, source_target_pairs={{0,1},{1,0},{2,3},{3,2},{4,5},{5,4},{6,7},{7,6},{8,9},{9,8},{10,11... | collective-permute-start | bytes 786440 | tf_op jit(solution)/shard_map/ppermute | solution.py:42
  74.6 1.2 %collective-permute-done.4.other_ref = bf16[128,1024]{1,0:T(8,128)(2,1)S(1)} collective-permute-done((bf16[128,1024]{1,0:T(8,128)(2,1)S(1)}, bf16[128,1024]{1,0:T(8,128)(2,1)S(1)}, u32[]{:S(2)}, u32[]{:S(2)}) %collective-permute-start.4) | collective-permute-done | bytes 262176 | tf_op jit(solution)/shard_map/ppermute | solution.py:42
  75.7 0.0 copy-done.10
  75.7 0.0 copy-done.8
  75.7 1.1 %finish.1 = bf16[64,1024]{1,0:T(8,128)(2,1)} custom-call(s32[1]{0:T(128)} %bitcast.core_ref, f32[128,1024]{1,0:T(8,128)S(1)} %get-tuple-element.20.mine_ref, bf16[128,1024]{1,0:T(8,128)(2,1)S(1)} %collective-permute-done.4.other_ref, bf16[64,2048]{1,0:T(8,128)(2,1)S(1)} %copy-done.8, f32[1,1024]{1,0:T(1,128)S(1)} %bitcast.20), custom_call_target="tpu_custom_call" | custom-call | flops 10000000 | bytes 2000000 | tf_op jit(solution)/shard_map/finish/pallas_call | solution.py:374
  (3 shorter events, 0.0 us)
Async XLA Ops:
  0.6 12.0 %copy-start = (bf16[1,2048,256]{2,1,0:T(8,128)(2,1)S(1)}, bf16[1,2048,256]{2,1,0:T(8,128)(2,1)}, u32[]{:S(2)}) copy-start(bf16[1,2048,256]{2,1,0:T(8,128)(2,1)} %param.31) | copy-start | bytes 3145732
  0.6 12.1 %copy-start.1 = (bf16[1,2048,256]{2,1,0:T(8,128)(2,1)S(1)}, bf16[1,2048,256]{2,1,0:T(8,128)(2,1)}, u32[]{:S(2)}) copy-start(bf16[1,2048,256]{2,1,0:T(8,128)(2,1)} %param.32) | copy-start | bytes 3145732
  0.7 12.6 %copy-start.14 = (s32[64,4]{0,1:T(4,128)S(1)}, s32[64,4]{0,1:T(4,128)}, u32[]{:S(2)}) copy-start(s32[64,4]{0,1:T(4,128)} %param.30) | copy-start | bytes 3076
  0.7 13.2 %copy-start.4 = (bf16[64,2048]{1,0:T(8,128)(2,1)S(1)}, bf16[64,2048]{1,0:T(8,128)(2,1)}, u32[]{:S(2)}) copy-start(bf16[64,2048]{1,0:T(8,128)(2,1)} %x_ref.3) | copy-start | bytes 786436
  0.7 13.1 %copy-start.9 = (f32[2048]{0:T(1024)S(1)}, f32[2048]{0:T(1024)}, u32[]{:S(2)}) copy-start(f32[2048]{0:T(1024)} %param.28) | copy-start | bytes 24580
  11.2 2.6 %collective-permute-start = (bf16[64,2048]{1,0:T(8,128)(2,1)S(1)}, bf16[64,2048]{1,0:T(8,128)(2,1)S(1)}, u32[]{:S(2)}, u32[]{:S(2)}) collective-permute-start(bf16[64,2048]{1,0:T(8,128)(2,1)S(1)} %attend.1.own_ref), channel_id=1, source_target_pairs={{0,1},{1,0},{2,3},{3,2},{4,5},{5,4},{6,7},{7,6},{8,9},{9,8},{10,11... | collective-permute-start | bytes 786440 | tf_op jit(solution)/shard_map/ppermute | solution.py:42
  12.7 22.9 %collective-permute-start.1 = (bf16[2048,256]{1,0:T(8,128)(2,1)S(1)}, bf16[2048,256]{1,0:T(8,128)(2,1)}, u32[]{:S(2)}, u32[]{:S(2)}) collective-permute-start(bf16[2048,256]{1,0:T(8,128)(2,1)S(1)} %bitcast.15), channel_id=1, source_target_pairs={{0,1},{1,0},{2,3},{3,2},{4,5},{5,4},{6,7},{7,6},{8,9},{9,8},{10,11... | collective-permute-start | bytes 3145736 | tf_op jit(solution)/shard_map/ppermute | solution.py:42
  12.8 22.8 %collective-permute-start.2 = (bf16[2048,256]{1,0:T(8,128)(2,1)S(1)}, bf16[2048,256]{1,0:T(8,128)(2,1)}, u32[]{:S(2)}, u32[]{:S(2)}) collective-permute-start(bf16[2048,256]{1,0:T(8,128)(2,1)S(1)} %bitcast.17), channel_id=1, source_target_pairs={{0,1},{1,0},{2,3},{3,2},{4,5},{5,4},{6,7},{7,6},{8,9},{9,8},{10,11... | collective-permute-start | bytes 3145736 | tf_op jit(solution)/shard_map/ppermute | solution.py:42
  13.2 22.4 %collective-permute-start.3 = (bf16[256,2048]{1,0:T(8,128)(2,1)}, bf16[256,2048]{1,0:T(8,128)(2,1)}, u32[]{:S(2)}, u32[]{:S(2)}) collective-permute-start(bf16[256,2048]{1,0:T(8,128)(2,1)} %bitcast.11.refs_2_), channel_id=1, source_target_pairs={{0,1},{1,0},{2,3},{3,2},{4,5},{5,4},{6,7},{7,6},{8,9},{9,8},{10,11... | collective-permute-start | bytes 3145736 | tf_op jit(solution)/shard_map/ppermute | solution.py:42
  13.7 2.4 %copy-start.12 = (f32[64,128]{1,0:T(8,128)}, f32[64,128]{1,0:T(8,128)S(1)}, u32[]{:S(2)}) copy-start(f32[64,128]{1,0:T(8,128)S(1)} %get-tuple-element.15.member_ref) | copy-start | bytes 98308
  16.1 29.4 %all-to-all-start = ((bf16[64,8,1024]{2,1,0:T(8,128)(2,1)}), bf16[64,8,1024]{2,1,0:T(8,128)(2,1)S(1)}, u32[]{:S(2)}, u32[]{:S(2)}) async-start(bf16[64,8,1024]{2,1,0:T(8,128)(2,1)} %bitcast.8), calls=%async_computation | async-start | bytes 2097152 | tf_op jit(solution)/shard_map/all_to_all | solution.py:418
  27.3 1.0 %copy-start.7 = (bf16[64,2048]{1,0:T(8,128)(2,1)S(1)}, bf16[64,2048]{1,0:T(8,128)(2,1)}, u32[]{:S(2)}) copy-start(bf16[64,2048]{1,0:T(8,128)(2,1)} %get-tuple-element.14.hidden_ref) | copy-start | bytes 786436
  28.3 0.9 %copy-start.11 = (bf16[2048,64]{0,1:T(8,128)(2,1)S(1)}, bf16[2048,64]{0,1:T(8,128)(2,1)}, u32[]{:S(2)}) copy-start(bf16[2048,64]{0,1:T(8,128)(2,1)} %param.29) | copy-start | bytes 786436
  29.2 0.8 copy-start.13
  34.0 0.8 %copy-start.2 = (f32[64,2048]{1,0:T(8,128)}, f32[64,2048]{1,0:T(8,128)S(1)}, u32[]{:S(2)}) copy-start(f32[64,2048]{1,0:T(8,128)S(1)} %get-tuple-element.19.shared_ref) | copy-start | bytes 1572868
  34.8 0.7 copy-start.5
  35.6 40.2 %copy-start.10 = (f32[1024]{0:T(1024)S(1)}, f32[1024]{0:T(1024)}, u32[]{:S(2)}) copy-start(f32[1024]{0:T(1024)} %param.37) | copy-start | bytes 12292
  35.6 35.3 %copy-start.6 = (bf16[256,512]{1,0:T(8,128)(2,1)S(1)}, bf16[256,512]{1,0:T(8,128)(2,1)}, u32[]{:S(2)}) copy-start(bf16[256,512]{1,0:T(8,128)(2,1)} %copy-done.5) | copy-start | bytes 786436
  45.4 25.5 %copy-start.3 = (f32[64,2048]{1,0:T(8,128)S(1)}, f32[64,2048]{1,0:T(8,128)}, u32[]{:S(2)}) copy-start(f32[64,2048]{1,0:T(8,128)} %copy-done.2) | copy-start | bytes 1572868
  45.4 30.3 %copy-start.8 = (bf16[64,2048]{1,0:T(8,128)(2,1)S(1)}, bf16[64,2048]{1,0:T(8,128)(2,1)}, u32[]{:S(2)}) copy-start(bf16[64,2048]{1,0:T(8,128)(2,1)} %get-tuple-element.14.hidden_ref) | copy-start | bytes 786436
  71.3 4.4 %collective-permute-start.4 = (bf16[128,1024]{1,0:T(8,128)(2,1)S(1)}, bf16[128,1024]{1,0:T(8,128)(2,1)S(1)}, u32[]{:S(2)}, u32[]{:S(2)}) collective-permute-start(bf16[128,1024]{1,0:T(8,128)(2,1)S(1)} %get-tuple-element.21), channel_id=1, source_target_pairs={{0,1},{1,0},{2,3},{3,2},{4,5},{5,4},{6,7},{7,6},{8,9},{9,8},{10,11... | collective-permute-start | bytes 786440 | tf_op jit(solution)/shard_map/ppermute | solution.py:42

commit v2 on v1

--- a/solution.py
+++ b/solution.py
@@ -13,9 +13,11 @@
 F32 = jnp.float32
 BF16 = jnp.bfloat16
 VMEM = pltpu.VMEM
-SEQ_STEP = 8
+SEQ_STEP = 16
 CUM = 256
-AHEAD = 3
+COLUMNS = 256
+PIECES = 4
+AHEAD = 2
 
 
 def iota(shape, dim):
@@ -215,7 +217,7 @@
 
 
 def dispatch_kernel(
-    x_ref, own_ref, other_ref, gain_ref, place_ref, hidden_hbm, out_ref, hidden_scr, sem
+    x_ref, own_ref, other_ref, gain_ref, place_ref, hidden_hbm, out_hbm, hidden_scr, out_scr, sems
 ):
     v = (
         RESIDUAL_SCALE * x_ref[...].astype(F32)
@@ -226,10 +228,17 @@
     var = jnp.mean(centered * centered, axis=1, keepdims=True)
     hidden = (centered * lax.rsqrt(var + NORM_EPS) * gain_ref[...]).astype(BF16)
     hidden_scr[...] = hidden
-    copy = pltpu.make_async_copy(hidden_scr, hidden_hbm, sem)
-    copy.start()
-    out_ref[...] = dot(place_ref[...], halves(hidden)).astype(BF16)
-    copy.wait()
+    copies = [pltpu.make_async_copy(hidden_scr, hidden_hbm, sems.at[PIECES])]
+    stacked = halves(hidden)
+    rows = out_scr.shape[0] // PIECES
+    for i in range(PIECES):
+        part = pl.ds(i * rows, rows)
+        out_scr[part, :] = dot(place_ref[part, :], stacked).astype(BF16)
+        copies.append(pltpu.make_async_copy(out_scr.at[part], out_hbm.at[part], sems.at[i]))
+        copies[-1].start()
+    copies[0].start()
+    for copy in copies:
+        copy.wait()
 
 
 def dispatch(inputs, own, other, gain, placement):
@@ -238,11 +247,15 @@
         dispatch_kernel,
         out_shape=(
             pltpu.HBM((seqs, width), BF16),
-            jax.ShapeDtypeStruct((placement.shape[0], width // 2), BF16),
+            pltpu.HBM((placement.shape[0], width // 2), BF16),
         ),
         in_specs=[whole()] * 5,
-        out_specs=(pl.BlockSpec(memory_space=pltpu.HBM), whole()),
-        scratch_shapes=[VMEM((seqs, width), BF16), pltpu.SemaphoreType.DMA],
+        out_specs=(pl.BlockSpec(memory_space=pltpu.HBM),) * 2,
+        scratch_shapes=[
+            VMEM((seqs, width), BF16),
+            VMEM((placement.shape[0], width // 2), BF16),
+            pltpu.SemaphoreType.DMA((PIECES + 1,)),
+        ],
         compiler_params=pltpu.CompilerParams(vmem_limit_bytes=12 * 2**20),
         cost_estimate=pl.CostEstimate(flops=2 * 10**8, bytes_accessed=2 * 10**6, transcendentals=64),
         name="dispatch",
@@ -250,12 +263,25 @@
 
 
 def local_kernel(
-    hidden_ref, x_ref, router_ref, member_ref, place_ref, sg_ref, su_ref, sd_ref, wk_ref, wv_ref,
-    shared_ref, weight_ref, nk_ref, nv_ref,
+    hidden_hbm, x_hbm, router_hbm, member_ref, place_ref, sg_hbm, su_hbm, sd_hbm, wk_hbm, wv_hbm,
+    shared_ref, weight_ref, nk_ref, nv_ref, *scratch,
 ):
+    *buffers, sems = scratch
+    sources = [hidden_hbm, sg_hbm, su_hbm, sd_hbm, router_hbm, x_hbm, wk_hbm, wv_hbm]
+    copies = [
+        pltpu.make_async_copy(src, dst, sems.at[i])
+        for i, (src, dst) in enumerate(zip(sources, buffers))
+    ]
+    for copy in copies:
+        copy.start()
+    hidden_ref, sg_ref, su_ref, sd_ref, router_ref, x_ref, wk_ref, wv_ref = buffers
+    for copy in copies[:3]:
+        copy.wait()
     hidden = hidden_ref[...]
     gate, up = dot(hidden, sg_ref[...]), dot(hidden, su_ref[...])
     inner = (gate / (1.0 + jnp.exp(-gate)) * up).astype(BF16)
+    for copy in copies[3:]:
+        copy.wait()
     shared_ref[...] = dot(inner, sd_ref[...])
     probs = 1.0 / (1.0 + jnp.exp(-dot_nt(router_ref[...], hidden)))
     probs = jnp.concatenate([probs, probs], axis=1) * member_ref[...]
@@ -278,6 +304,8 @@
     seqs, width = hidden.shape
     rows, lanes = placement.shape
     size = wk_t.shape[0]
+    any_space = pl.BlockSpec(memory_space=pl.ANY)
+    buffered = [hidden, sg, su, sd, router_t, inputs, wk_t, wv_t]
     return pl.pallas_call(
         local_kernel,
         out_shape=(
@@ -286,18 +314,32 @@
             jax.ShapeDtypeStruct((seqs, size), BF16),
             jax.ShapeDtypeStruct((seqs, size), BF16),
         ),
-        in_specs=[whole()] * 10,
+        in_specs=[any_space] * 3 + [whole()] * 2 + [any_space] * 5,
         out_specs=(whole(),) * 4,
-        compiler_params=pltpu.CompilerParams(vmem_limit_bytes=20 * 2**20),
+        scratch_shapes=[VMEM(b.shape, b.dtype) for b in buffered]
+        + [pltpu.SemaphoreType.DMA((len(buffered),))],
+        compiler_params=pltpu.CompilerParams(vmem_limit_bytes=24 * 2**20),
         cost_estimate=pl.CostEstimate(
             flops=4 * 10**9, bytes_accessed=5 * 10**6, transcendentals=10**5
         ),
         name="local",
-    )(hidden, inputs, router_t, member, placement, *in_hbm(sg, su, sd, wk_t, wv_t))
-
-
-def expert_kernel(order_ref, rows_ref, *refs):
-    weights, out_ref = refs[:-1], refs[-1]
+    )(
+        *in_hbm(hidden, inputs, router_t), member, placement, *in_hbm(sg, su, sd, wk_t, wv_t)
+    )
+
+
+def expert_kernel(
+    order_ref, rows_ref, own_gate_ref, own_up_ref, down_hbm, gate2_hbm, up2_hbm, down2_hbm, out_ref,
+    down_scr, gate2_scr, up2_scr, down2_scr, sems,
+):
+    sources = [gate2_hbm, up2_hbm, down_hbm, down2_hbm]
+    buffers = [gate2_scr, up2_scr, down_scr, down2_scr]
+    gate_copy, up_copy, *down_copies = [
+        pltpu.make_async_copy(src, dst, sems.at[i])
+        for i, (src, dst) in enumerate(zip(sources, buffers))
+    ]
+    gate_copy.start()
+    up_copy.start()
     groups, lines, half = rows_ref.shape
     slots = lines // 2
     low = iota((groups // 2, lines, half), 1) < slots
@@ -306,33 +348,56 @@
     count = groups * slots
     first = jnp.where(low, a, pltpu.roll(b, slots, 1)).reshape(count, half).astype(BF16)
     second = jnp.where(low, pltpu.roll(a, slots, 1), b).reshape(count, half).astype(BF16)
-    total = None
-    for i in range(2):
-        gate_ref, up_ref, down_ref = weights[3 * i : 3 * i + 3]
-        gate = dot(first, gate_ref[:half, :]) + dot(second, gate_ref[half:, :])
-        up = dot(first, up_ref[:half, :]) + dot(second, up_ref[half:, :])
-        inner = (gate / (1.0 + jnp.exp(-gate)) * up).astype(BF16)
-        part = dot(inner, down_ref[...]).astype(BF16).astype(F32)
-        total = part if total is None else total + part
-    a = total[:, :half].reshape(groups // 2, lines, half)
-    b = total[:, half:].reshape(groups // 2, lines, half)
-    even = jnp.where(low, a, pltpu.roll(b, slots, 1))
-    odd = jnp.where(low, pltpu.roll(a, slots, 1), b)
-    out_ref[...] = jnp.stack([even, odd], axis=1).reshape(groups, lines, half).astype(BF16)
+
+    def product(ref):
+        return dot(first, ref[:half, :]) + dot(second, ref[half:, :])
+
+    def gated(gate, up):
+        return (gate / (1.0 + jnp.exp(-gate)) * up).astype(BF16)
+
+    gate, up = product(own_gate_ref), product(own_up_ref)
+    for copy in down_copies:
+        copy.start()
+    own = gated(gate, up)
+    gate_copy.wait()
+    up_copy.wait()
+    other = gated(product(gate2_scr), product(up2_scr))
+    for copy in down_copies:
+        copy.wait()
+
+    def result(start):
+        cols = slice(start, start + COLUMNS)
+        parts = [
+            dot(inner, ref[:, cols]).astype(BF16).astype(F32)
+            for inner, ref in ((own, down_scr), (other, down2_scr))
+        ]
+        return (parts[0] + parts[1]).reshape(groups // 2, lines, COLUMNS)
+
+    low = iota((groups // 2, lines, COLUMNS), 1) < slots
+    for start in range(0, half, COLUMNS):
+        a, b = result(start), result(half + start)
+        even = jnp.where(low, a, pltpu.roll(b, slots, 1))
+        odd = jnp.where(low, pltpu.roll(a, slots, 1), b)
+        both = jnp.stack([even, odd], axis=1).reshape(groups, lines, COLUMNS)
+        out_ref[:, :, start : start + COLUMNS] = both.astype(BF16)
 
 
 def expert(order, rows, weights):
+    gate, up, *streamed = weights
+    any_space = pl.BlockSpec(memory_space=pl.ANY)
     return pl.pallas_call(
         expert_kernel,
         out_shape=jax.ShapeDtypeStruct(rows.shape, BF16),
-        in_specs=[pl.BlockSpec(memory_space=pl.ANY)] + [whole()] * 7,
+        in_specs=[any_space] + [whole()] * 3 + [any_space] * 4,
         out_specs=whole(),
+        scratch_shapes=[VMEM(w.shape, w.dtype) for w in streamed]
+        + [pltpu.SemaphoreType.DMA((len(streamed),))],
         compiler_params=pltpu.CompilerParams(vmem_limit_bytes=32 * 2**20),
         cost_estimate=pl.CostEstimate(
             flops=2 * 10**9, bytes_accessed=8 * 10**6, transcendentals=3 * 10**5
         ),
         name="expert",
-    )(*in_hbm(order), rows, *weights)
+    )(*in_hbm(order), rows, gate, up, *in_hbm(*streamed))
 
 
 def combine_kernel(weight_ref, rows_ref, shared_ref, mine_ref, send_ref):

time: 77.2 us -> 73.8 us (0.956)
  Pallas kernels: 23.1 us -> 19.6 us
  waiting for transfers between devices: 11.1 us -> 13.9 us
  local copies, waits for them, and re-layouts: 4.21 us -> 1.58 us
    all_to_all x1, waiting for transfers between devices: 9.85 us -> 12.6 us  [on_device(): lax.all_to_all(outgoing.reshape(experts, 2 * slots, width // 2), 'ep', 0,...]
    unnamed x30 -> x22, local copies, waits for them, and re-layouts: 4.21 us -> 1.58 us
    pallas_call x1, Pallas kernels: 10.5 us -> 8.72 us  [attend(): pl.pallas_call(attend_kernel, out_shape=jax.ShapeDtypeStruct((seqs, width...]
    pallas_call x1, Pallas kernels: 4.47 us -> 3.56 us  [expert(): pl.pallas_call(expert_kernel, out_shape=jax.ShapeDtypeStruct(rows.shape,...]
  transfers between devices with their start and end apart: 6 -> 6, of which waited for: 3 -> 3; matrix products, arithmetic and copies ran while one was open for 0% -> 0% of each run, Pallas kernels for 9% -> 8%
where the time goes in v2:
time: 73.8 us; the launch traced here: 73.5 us
  blocking collectives  21 us (28%)
  Pallas kernels  19.6 us (27%)
  starting transfers between devices  16.6 us (22%)
  waiting for transfers between devices  13.9 us (19%)
  local copies, waits for them, and re-layouts  1.58 us (2%)
  between operations  0.78 us (1%)
    all_to_all x1, blocking collectives, on_device(): returned = lax.all_to_all(results, 'ep', 0, 0, tiled=True)  21 us
    all_to_all x1, waiting for transfers between devices, on_device(): lax.all_to_all(outgoing.reshape(experts, 2 * slots, width // 2), 'ep', 0,...  12.6 us
    all_to_all x1, starting transfers between devices, on_device(): lax.all_to_all(outgoing.reshape(experts, 2 * slots, width // 2), 'ep', 0,...  11.3 us
    pallas_call x1, Pallas kernels, attend(): pl.pallas_call(attend_kernel, out_shape=jax.ShapeDtypeStruct((seqs, width...  8.72 us
    ppermute x5, starting transfers between devices, swapped(): return lax.ppermute(x, 'tp', [(0, 1), (1, 0)])  5.31 us
    pallas_call x1, Pallas kernels, local(): pl.pallas_call(local_kernel, out_shape=(jax.ShapeDtypeStruct((seqs, width...  3.85 us
    pallas_call x1, Pallas kernels, expert(): pl.pallas_call(expert_kernel, out_shape=jax.ShapeDtypeStruct(rows.shape,...  3.56 us
    pallas_call x1, Pallas kernels, dispatch(): pl.pallas_call(dispatch_kernel, out_shape=(pltpu.HBM((seqs, width), BF16)...  1.64 us
  transfers between devices with their start and end apart: 6, of which 3 were waited for; matrix products, arithmetic and copies ran while one was open for 0% of the time, Pallas kernels for 8%

profile of v2, /device:TPU:1, one launch (start us, length us, event | category | flops | bytes accessed | tf_op | source)
XLA Modules:
  0.0 73.5 jit_solution(3604114088982913166)
XLA Ops:
  0.6 0.0 copy-start
  0.6 0.0 copy-start.1
  0.7 0.0 copy-start.10
  0.7 0.0 copy-start.4
  0.7 0.0 copy-start.6
  0.7 8.7 %attend.1.own_ref = bf16[64,2048]{1,0:T(8,128)(2,1)S(1)} custom-call(s32[64]{0:T(128)} %len_hbm.1, f32[8]{0:T(128)} %bias_hbm.1, bf16[64,2048]{1,0:T(8,128)(2,1)} %x_hbm.3, bf16[2048,512]{1,0:T(8,128)(2,1)} %wq_hbm.1, bf16[64,64,1024]{2,1,0:T(8,128)(2,1)} %bitcast.23, bf16[64,64,1024]{2,1,0:T(8,128)(2,1)} %bitcast.24, bf16[512,2048]{1,0:T(8,128)(2,1)} %wo_hbm.1), custom_call_target="tpu_custom_call" | custom-call | flops 8000000000 | bytes 22000000 | tf_op jit(solution)/shard_map/attend/pallas_call | solution.py:145
  9.4 1.5 %collective-permute-start = (bf16[64,2048]{1,0:T(8,128)(2,1)S(1)}, bf16[64,2048]{1,0:T(8,128)(2,1)S(1)}, u32[]{:S(2)}, u32[]{:S(2)}) collective-permute-start(bf16[64,2048]{1,0:T(8,128)(2,1)S(1)} %attend.1.own_ref), channel_id=1, source_target_pairs={{0,1},{1,0},{2,3},{3,2},{4,5},{5,4},{6,7},{7,6},{8,9},{9,8},{10,11... | collective-permute-start | bytes 786440 | tf_op jit(solution)/shard_map/ppermute | solution.py:44
  10.9 0.0 copy-done
  10.9 0.1 collective-permute-start.1
  11.0 0.0 copy-done.1
  11.0 0.4 collective-permute-start.2
  11.4 0.1 collective-permute-start.3
  11.5 0.0 copy-done.10
  11.5 0.1 pad_add_fusion.routes_ref
  11.6 0.3 place.1
  11.9 0.0 copy-start.8
  11.9 0.1 collective-permute-done.other_ref
  12.0 0.0 copy-done.4
  12.0 0.0 copy-done.6
  12.0 1.6 %dispatch.1 = (bf16[64,2048]{1,0:T(8,128)(2,1)}, bf16[512,1024]{1,0:T(8,128)(2,1)}) custom-call(bf16[64,2048]{1,0:T(8,128)(2,1)S(1)} %copy-done.4, bf16[64,2048]{1,0:T(8,128)(2,1)S(1)} %attend.1.own_ref, bf16[64,2048]{1,0:T(8,128)(2,1)S(1)} %collective-permute-done.other_ref, f32[1,2048]{1,0:T(1,128)S(1)} %bitcast.19, ...), custom_call_target="tpu_custom_call" | custom-call | flops 200000000 | bytes 2000000 | tf_op jit(solution)/shard_map/dispatch/pallas_call | solution.py:246
  13.7 0.0 copy-done.8
  13.7 11.3 %all-to-all-start = ((bf16[64,8,1024]{2,1,0:T(8,128)(2,1)}), bf16[64,8,1024]{2,1,0:T(8,128)(2,1)S(1)}, u32[]{:S(2)}, u32[]{:S(2)}) async-start(bf16[64,8,1024]{2,1,0:T(8,128)(2,1)} %bitcast.21), calls=%async_computation | async-start | bytes 2097152 | tf_op jit(solution)/shard_map/all_to_all | solution.py:483
  25.0 0.0 copy-start.9
  25.0 0.7 %copy-done.9 = f32[64,128]{1,0:T(8,128)S(1)} copy-done((f32[64,128]{1,0:T(8,128)S(1)}, f32[64,128]{1,0:T(8,128)}, u32[]{:S(2)}) %copy-start.9) | copy-done | bytes 32792
  25.7 3.9 %local.1 = (f32[64,2048]{1,0:T(8,128)S(1)}, bf16[256,512]{1,0:T(8,128)(2,1)S(1)}, bf16[64,64]{1,0:T(8,128)(2,1)}, bf16[64,64]{1,0:T(8,128)(2,1)}) custom-call(bf16[64,2048]{1,0:T(8,128)(2,1)} %get-tuple-element.14.hidden_hbm.hidden_ref, bf16[64,2048]{1,0:T(8,128)(2,1)} %x_hbm.3, bf16[64,2048]{1,0:T(8,128)(2,1)} %bitcast.25, f32[64,128]{1,0:T(8,128)S(1)} %copy-done.9, ...), custom_call_target="tpu_custom_call" | custom-call | flops 4000000000 | bytes 5000000 | tf_op jit(solution)/shard_map/local/pallas_call | solution.py:309
  29.6 0.0 copy-start.2
  29.6 0.8 %copy-done.2 = f32[64,2048]{1,0:T(8,128)} copy-done((f32[64,2048]{1,0:T(8,128)}, f32[64,2048]{1,0:T(8,128)S(1)}, u32[]{:S(2)}) %copy-start.2) | copy-done | bytes 524312
  30.4 0.0 copy-start.7
  30.4 0.0 collective-permute-done.1.gate2_hbm
  30.4 0.0 collective-permute-done.2.up2_hbm
  30.4 0.0 collective-permute-done.3.down2_hbm
  30.4 12.6 %all-to-all-done.rows_ref = bf16[64,8,1024]{2,1,0:T(8,128)(2,1)S(1)} async-done(((bf16[64,8,1024]{2,1,0:T(8,128)(2,1)}), bf16[64,8,1024]{2,1,0:T(8,128)(2,1)S(1)}, u32[]{:S(2)}, u32[]{:S(2)}) %all-to-all-start) | async-done | bytes 1048608 | tf_op jit(solution)/shard_map/all_to_all | solution.py:483
  43.1 0.0 copy-start.3
  43.1 0.0 copy-start.5
  43.1 3.6 %expert.1 = bf16[64,8,1024]{2,1,0:T(8,128)(2,1)S(1)} custom-call(bf16[64,64]{1,0:T(8,128)(2,1)} %get-tuple-element.11.order_ref, bf16[64,8,1024]{2,1,0:T(8,128)(2,1)S(1)} %all-to-all-done.rows_ref, bf16[2048,256]{1,0:T(8,128)(2,1)S(1)} %bitcast.16, bf16[2048,256]{1,0:T(8,128)(2,1)S(1)} %bitcast.18, bf16[256,2048]{1,0:T(8,128)(2,1)} %bitcast.11.down_hbm, ...), custom_call_target="tpu_custom_call" | custom-call | flops 2000000000 | bytes 8000000 | tf_op jit(solution)/shard_map/expert/pallas_call | solution.py:388
  46.6 21.0 %all_to_all.10 = bf16[64,8,1024]{2,1,0:T(8,128)(2,1)S(1)} all-to-all(bf16[64,8,1024]{2,1,0:T(8,128)(2,1)S(1)} %expert.1), channel_id=1, replica_groups=mesh['ep'=64,'tp'=2] {'ep'}, dimensions={0} | all-to-all | bytes 2097152 | tf_op jit(solution)/shard_map/all_to_all | solution.py:493
  67.6 0.0 copy-done.3
  67.6 0.4 combine.1
  68.1 3.2 %collective-permute-start.4 = (bf16[128,1024]{1,0:T(8,128)(2,1)S(1)}, bf16[128,1024]{1,0:T(8,128)(2,1)S(1)}, u32[]{:S(2)}, u32[]{:S(2)}) collective-permute-start(bf16[128,1024]{1,0:T(8,128)(2,1)S(1)} %get-tuple-element.21), channel_id=1, source_target_pairs={{0,1},{1,0},{2,3},{3,2},{4,5},{5,4},{6,7},{7,6},{8,9},{9,8},{10,11... | collective-permute-start | bytes 786440 | tf_op jit(solution)/shard_map/ppermute | solution.py:44
  71.3 1.2 %collective-permute-done.4.other_ref = bf16[128,1024]{1,0:T(8,128)(2,1)S(1)} collective-permute-done((bf16[128,1024]{1,0:T(8,128)(2,1)S(1)}, bf16[128,1024]{1,0:T(8,128)(2,1)S(1)}, u32[]{:S(2)}, u32[]{:S(2)}) %collective-permute-start.4) | collective-permute-done | bytes 262176 | tf_op jit(solution)/shard_map/ppermute | solution.py:44
  72.5 0.0 copy-done.7
  72.5 0.0 copy-done.5
  72.5 1.1 %finish.1 = bf16[64,1024]{1,0:T(8,128)(2,1)} custom-call(s32[1]{0:T(128)} %bitcast.core_ref, f32[128,1024]{1,0:T(8,128)S(1)} %get-tuple-element.20.mine_ref, bf16[128,1024]{1,0:T(8,128)(2,1)S(1)} %collective-permute-done.4.other_ref, bf16[64,2048]{1,0:T(8,128)(2,1)S(1)} %copy-done.5, f32[1,1024]{1,0:T(1,128)S(1)} %bitcast.20), custom_call_target="tpu_custom_call" | custom-call | flops 10000000 | bytes 2000000 | tf_op jit(solution)/shard_map/finish/pallas_call | solution.py:439
Async XLA Ops:
  0.6 10.2 %copy-start = (bf16[1,2048,256]{2,1,0:T(8,128)(2,1)S(1)}, bf16[1,2048,256]{2,1,0:T(8,128)(2,1)}, u32[]{:S(2)}) copy-start(bf16[1,2048,256]{2,1,0:T(8,128)(2,1)} %param.31) | copy-start | bytes 3145732
  0.6 10.3 %copy-start.1 = (bf16[1,2048,256]{2,1,0:T(8,128)(2,1)S(1)}, bf16[1,2048,256]{2,1,0:T(8,128)(2,1)}, u32[]{:S(2)}) copy-start(bf16[1,2048,256]{2,1,0:T(8,128)(2,1)} %param.32) | copy-start | bytes 3145732
  0.7 10.8 %copy-start.10 = (s32[64,4]{0,1:T(4,128)S(1)}, s32[64,4]{0,1:T(4,128)}, u32[]{:S(2)}) copy-start(s32[64,4]{0,1:T(4,128)} %param.30) | copy-start | bytes 3076
  0.7 11.4 %copy-start.4 = (bf16[64,2048]{1,0:T(8,128)(2,1)S(1)}, bf16[64,2048]{1,0:T(8,128)(2,1)}, u32[]{:S(2)}) copy-start(bf16[64,2048]{1,0:T(8,128)(2,1)} %x_hbm.3) | copy-start | bytes 786436
  0.7 11.4 %copy-start.6 = (f32[2048]{0:T(1024)S(1)}, f32[2048]{0:T(1024)}, u32[]{:S(2)}) copy-start(f32[2048]{0:T(1024)} %param.28) | copy-start | bytes 24580
  9.4 2.6 %collective-permute-start = (bf16[64,2048]{1,0:T(8,128)(2,1)S(1)}, bf16[64,2048]{1,0:T(8,128)(2,1)S(1)}, u32[]{:S(2)}, u32[]{:S(2)}) collective-permute-start(bf16[64,2048]{1,0:T(8,128)(2,1)S(1)} %attend.1.own_ref), channel_id=1, source_target_pairs={{0,1},{1,0},{2,3},{3,2},{4,5},{5,4},{6,7},{7,6},{8,9},{9,8},{10,11... | collective-permute-start | bytes 786440 | tf_op jit(solution)/shard_map/ppermute | solution.py:44
  10.9 19.5 %collective-permute-start.1 = (bf16[2048,256]{1,0:T(8,128)(2,1)S(1)}, bf16[2048,256]{1,0:T(8,128)(2,1)}, u32[]{:S(2)}, u32[]{:S(2)}) collective-permute-start(bf16[2048,256]{1,0:T(8,128)(2,1)S(1)} %bitcast.15), channel_id=1, source_target_pairs={{0,1},{1,0},{2,3},{3,2},{4,5},{5,4},{6,7},{7,6},{8,9},{9,8},{10,11... | collective-permute-start | bytes 3145736 | tf_op jit(solution)/shard_map/ppermute | solution.py:44
  11.0 19.4 %collective-permute-start.2 = (bf16[2048,256]{1,0:T(8,128)(2,1)S(1)}, bf16[2048,256]{1,0:T(8,128)(2,1)}, u32[]{:S(2)}, u32[]{:S(2)}) collective-permute-start(bf16[2048,256]{1,0:T(8,128)(2,1)S(1)} %bitcast.17), channel_id=1, source_target_pairs={{0,1},{1,0},{2,3},{3,2},{4,5},{5,4},{6,7},{7,6},{8,9},{9,8},{10,11... | collective-permute-start | bytes 3145736 | tf_op jit(solution)/shard_map/ppermute | solution.py:44
  11.4 19.0 %collective-permute-start.3 = (bf16[256,2048]{1,0:T(8,128)(2,1)}, bf16[256,2048]{1,0:T(8,128)(2,1)}, u32[]{:S(2)}, u32[]{:S(2)}) collective-permute-start(bf16[256,2048]{1,0:T(8,128)(2,1)} %bitcast.11.down_hbm), channel_id=1, source_target_pairs={{0,1},{1,0},{2,3},{3,2},{4,5},{5,4},{6,7},{7,6},{8,9},{9,8},{10,11... | collective-permute-start | bytes 3145736 | tf_op jit(solution)/shard_map/ppermute | solution.py:44
  11.9 1.8 %copy-start.8 = (f32[64,128]{1,0:T(8,128)}, f32[64,128]{1,0:T(8,128)S(1)}, u32[]{:S(2)}) copy-start(f32[64,128]{1,0:T(8,128)S(1)} %get-tuple-element.15.member_ref) | copy-start | bytes 98308
  13.7 29.4 %all-to-all-start = ((bf16[64,8,1024]{2,1,0:T(8,128)(2,1)}), bf16[64,8,1024]{2,1,0:T(8,128)(2,1)S(1)}, u32[]{:S(2)}, u32[]{:S(2)}) async-start(bf16[64,8,1024]{2,1,0:T(8,128)(2,1)} %bitcast.21), calls=%async_computation | async-start | bytes 2097152 | tf_op jit(solution)/shard_map/all_to_all | solution.py:483
  25.0 0.8 %copy-start.9 = (f32[64,128]{1,0:T(8,128)S(1)}, f32[64,128]{1,0:T(8,128)}, u32[]{:S(2)}) copy-start(f32[64,128]{1,0:T(8,128)} %copy-done.8) | copy-start | bytes 98308
  29.6 0.8 %copy-start.2 = (f32[64,2048]{1,0:T(8,128)}, f32[64,2048]{1,0:T(8,128)S(1)}, u32[]{:S(2)}) copy-start(f32[64,2048]{1,0:T(8,128)S(1)} %get-tuple-element.19.shared_ref) | copy-start | bytes 1572868
  30.4 42.1 %copy-start.7 = (f32[1024]{0:T(1024)S(1)}, f32[1024]{0:T(1024)}, u32[]{:S(2)}) copy-start(f32[1024]{0:T(1024)} %param.37) | copy-start | bytes 12292
  43.1 24.6 %copy-start.3 = (f32[64,2048]{1,0:T(8,128)S(1)}, f32[64,2048]{1,0:T(8,128)}, u32[]{:S(2)}) copy-start(f32[64,2048]{1,0:T(8,128)} %copy-done.2) | copy-start | bytes 1572868
  43.1 29.4 %copy-start.5 = (bf16[64,2048]{1,0:T(8,128)(2,1)S(1)}, bf16[64,2048]{1,0:T(8,128)(2,1)}, u32[]{:S(2)}) copy-start(bf16[64,2048]{1,0:T(8,128)(2,1)} %get-tuple-element.14.hidden_hbm.hidden_ref) | copy-start | bytes 786436
  68.1 4.4 %collective-permute-start.4 = (bf16[128,1024]{1,0:T(8,128)(2,1)S(1)}, bf16[128,1024]{1,0:T(8,128)(2,1)S(1)}, u32[]{:S(2)}, u32[]{:S(2)}) collective-permute-start(bf16[128,1024]{1,0:T(8,128)(2,1)S(1)} %get-tuple-element.21), channel_id=1, source_target_pairs={{0,1},{1,0},{2,3},{3,2},{4,5},{5,4},{6,7},{7,6},{8,9},{9,8},{10,11... | collective-permute-start | bytes 786440 | tf_op jit(solution)/shard_map/ppermute | solution.py:44

commit v3 on v2

--- a/solution.py
+++ b/solution.py
@@ -229,6 +229,7 @@
     hidden = (centered * lax.rsqrt(var + NORM_EPS) * gain_ref[...]).astype(BF16)
     hidden_scr[...] = hidden
     copies = [pltpu.make_async_copy(hidden_scr, hidden_hbm, sems.at[PIECES])]
+    copies[0].start()
     stacked = halves(hidden)
     rows = out_scr.shape[0] // PIECES
     for i in range(PIECES):
@@ -236,7 +237,6 @@
         out_scr[part, :] = dot(place_ref[part, :], stacked).astype(BF16)
         copies.append(pltpu.make_async_copy(out_scr.at[part], out_hbm.at[part], sems.at[i]))
         copies[-1].start()
-    copies[0].start()
     for copy in copies:
         copy.wait()
 
@@ -400,52 +400,52 @@
     )(*in_hbm(order), rows, gate, up, *in_hbm(*streamed))
 
 
-def combine_kernel(weight_ref, rows_ref, shared_ref, mine_ref, send_ref):
+def combine_kernel(weight_ref, rows_ref, shared_ref, hidden_ref, mine_ref, send_ref):
     lanes = weight_ref.shape[0] // 2
     both = dot(weight_ref[...], rows_ref[...])
     part = both[:lanes, :] + both[lanes:, :] + halves(shared_ref[...])
-    mine_ref[...] = part
     send_ref[...] = part.astype(BF16)
-
-
-def combine(weight, rows, shared):
+    mine_ref[...] = part + RESIDUAL_SCALE * halves(hidden_ref[...]).astype(F32)
+
+
+def combine(weight, rows, shared, hidden):
     shape = (weight.shape[0] // 2, rows.shape[1])
     return pl.pallas_call(
         combine_kernel,
         out_shape=(jax.ShapeDtypeStruct(shape, F32), jax.ShapeDtypeStruct(shape, BF16)),
-        in_specs=[whole()] * 3,
+        in_specs=[whole()] * 4,
         out_specs=(whole(), whole()),
         compiler_params=pltpu.CompilerParams(vmem_limit_bytes=16 * 2**20),
         cost_estimate=pl.CostEstimate(flops=3 * 10**8, bytes_accessed=3 * 10**6, transcendentals=0),
         name="combine",
-    )(weight, rows, shared)
-
-
-def finish_kernel(core_ref, mine_ref, other_ref, hidden_ref, gain_ref, out_ref, mixed):
+    )(weight, rows, shared, hidden)
+
+
+def finish_kernel(core_ref, mine_ref, other_ref, gain_ref, out_ref):
     seqs, half = out_ref.shape
-    v = mine_ref[...] + other_ref[...].astype(F32) + RESIDUAL_SCALE * halves(hidden_ref[...]).astype(F32)
-    mixed[...] = v
+    width = 2 * half
+    v = mine_ref[...] + other_ref[...].astype(F32)
     sums = jnp.sum(v, axis=1, keepdims=True)
-    mean = (sums[:seqs] + sums[seqs:]) / (2 * half)
-    centered = v - jnp.concatenate([mean, mean], axis=0)
-    squares = jnp.sum(centered * centered, axis=1, keepdims=True)
-    scale = lax.rsqrt((squares[:seqs] + squares[seqs:]) / (2 * half) + NORM_EPS)
-    own = mixed[pl.ds(pl.multiple_of(core_ref[0] * seqs, seqs), seqs), :]
+    squares = jnp.sum(v * v, axis=1, keepdims=True)
+    mean = (sums[:seqs] + sums[seqs:]) / width
+    var = (squares[:seqs] + squares[seqs:]) / width - mean * mean
+    scale = lax.rsqrt(var + NORM_EPS)
+    rows = pl.ds(pl.multiple_of(core_ref[0] * seqs, seqs), seqs)
+    own = mine_ref[rows, :] + other_ref[rows, :].astype(F32)
     out_ref[...] = ((own - mean) * scale * gain_ref[...]).astype(BF16)
 
 
-def finish(core, mine, other, hidden, gain):
+def finish(core, mine, other, gain):
     lanes, half = mine.shape
     return pl.pallas_call(
         finish_kernel,
         out_shape=jax.ShapeDtypeStruct((lanes // 2, half), BF16),
-        in_specs=[pl.BlockSpec(memory_space=pltpu.SMEM)] + [whole()] * 4,
+        in_specs=[pl.BlockSpec(memory_space=pltpu.SMEM)] + [whole()] * 3,
         out_specs=whole(),
-        scratch_shapes=[VMEM((lanes, half), F32)],
         compiler_params=pltpu.CompilerParams(vmem_limit_bytes=12 * 2**20),
         cost_estimate=pl.CostEstimate(flops=10**7, bytes_accessed=2 * 10**6, transcendentals=64),
         name="finish",
-    )(core, mine, other, hidden, gain.reshape(1, half))
+    )(core, mine, other, gain.reshape(1, half))
 
 
 def on_device(
@@ -491,8 +491,8 @@
     )
     results = expert(new_keys, arrived, own_weights + other_weights)
     returned = lax.all_to_all(results, "ep", 0, 0, tiled=True)
-    mine, send = combine(weight, returned.reshape(experts * 2 * slots, width // 2), shared)
-    output = finish(core, mine, swapped(send), hidden, final_gain)
+    mine, send = combine(weight, returned.reshape(experts * 2 * slots, width // 2), shared, hidden)
+    output = finish(core, mine, swapped(send), final_gain)
     return (output, new_keys, new_values)
 
 

time: 73.8 us -> 73.5 us (level)
    unnamed x22 -> x26, local copies, waits for them, and re-layouts: 1.58 us -> 2.3 us
where the time goes in v3:
time: 73.5 us; the launch traced here: 73.2 us
  blocking collectives  21 us (29%)
  Pallas kernels  19.3 us (26%)
  starting transfers between devices  16.6 us (23%)
  waiting for transfers between devices  13.2 us (18%)
  local copies, waits for them, and re-layouts  2.3 us (3%)
  between operations  0.79 us (1%)
    all_to_all x1, blocking collectives, on_device(): returned = lax.all_to_all(results, 'ep', 0, 0, tiled=True)  21 us
    all_to_all x1, waiting for transfers between devices, on_device(): lax.all_to_all(outgoing.reshape(experts, 2 * slots, width // 2), 'ep', 0,...  11.9 us
    all_to_all x1, starting transfers between devices, on_device(): lax.all_to_all(outgoing.reshape(experts, 2 * slots, width // 2), 'ep', 0,...  11.3 us
    pallas_call x1, Pallas kernels, attend(): pl.pallas_call(attend_kernel, out_shape=jax.ShapeDtypeStruct((seqs, width...  8.72 us
    ppermute x5, starting transfers between devices, swapped(): return lax.ppermute(x, 'tp', [(0, 1), (1, 0)])  5.31 us
    pallas_call x1, Pallas kernels, local(): pl.pallas_call(local_kernel, out_shape=(jax.ShapeDtypeStruct((seqs, width...  3.85 us
    pallas_call x1, Pallas kernels, expert(): pl.pallas_call(expert_kernel, out_shape=jax.ShapeDtypeStruct(rows.shape,...  3.56 us
    unnamed x26, local copies, waits for them, and re-layouts  2.3 us
  transfers between devices with their start and end apart: 6, of which 3 were waited for; matrix products, arithmetic and copies ran while one was open for 0% of the time, Pallas kernels for 8%

profile of v3, /device:TPU:1, one launch (start us, length us, event | category | flops | bytes accessed | tf_op | source)
XLA Modules:
  0.0 73.2 jit_solution(15436041816302283579)
XLA Ops:
  0.6 0.0 copy-start
  0.6 0.0 copy-start.1
  0.7 0.0 copy-start.12
  0.7 0.0 copy-start.4
  0.7 0.0 copy-start.8
  0.7 8.7 %attend.1.own_ref = bf16[64,2048]{1,0:T(8,128)(2,1)S(1)} custom-call(s32[64]{0:T(128)} %len_hbm.1, f32[8]{0:T(128)} %bias_hbm.1, bf16[64,2048]{1,0:T(8,128)(2,1)} %x_hbm.3, bf16[2048,512]{1,0:T(8,128)(2,1)} %wq_hbm.1, bf16[64,64,1024]{2,1,0:T(8,128)(2,1)} %bitcast.23, bf16[64,64,1024]{2,1,0:T(8,128)(2,1)} %bitcast.24, bf16[512,2048]{1,0:T(8,128)(2,1)} %wo_hbm.1), custom_call_target="tpu_custom_call" | custom-call | flops 8000000000 | bytes 22000000 | tf_op jit(solution)/shard_map/attend/pallas_call | solution.py:145
  9.4 1.5 %collective-permute-start = (bf16[64,2048]{1,0:T(8,128)(2,1)S(1)}, bf16[64,2048]{1,0:T(8,128)(2,1)S(1)}, u32[]{:S(2)}, u32[]{:S(2)}) collective-permute-start(bf16[64,2048]{1,0:T(8,128)(2,1)S(1)} %attend.1.own_ref), channel_id=1, source_target_pairs={{0,1},{1,0},{2,3},{3,2},{4,5},{5,4},{6,7},{7,6},{8,9},{9,8},{10,11... | collective-permute-start | bytes 786440 | tf_op jit(solution)/shard_map/ppermute | solution.py:44
  10.9 0.0 copy-done
  10.9 0.1 collective-permute-start.1
  11.0 0.0 copy-done.1
  11.0 0.4 collective-permute-start.2
  11.4 0.1 collective-permute-start.3
  11.5 0.0 copy-done.12
  11.5 0.1 pad_add_fusion.routes_ref
  11.6 0.3 place.1
  11.9 0.0 copy-start.10
  11.9 0.1 collective-permute-done.other_ref
  12.0 0.0 copy-done.4
  12.0 0.0 copy-done.8
  12.0 1.5 %dispatch.1 = (bf16[64,2048]{1,0:T(8,128)(2,1)}, bf16[512,1024]{1,0:T(8,128)(2,1)}) custom-call(bf16[64,2048]{1,0:T(8,128)(2,1)S(1)} %copy-done.4, bf16[64,2048]{1,0:T(8,128)(2,1)S(1)} %attend.1.own_ref, bf16[64,2048]{1,0:T(8,128)(2,1)S(1)} %collective-permute-done.other_ref, f32[1,2048]{1,0:T(1,128)S(1)} %bitcast.19, ...), custom_call_target="tpu_custom_call" | custom-call | flops 200000000 | bytes 2000000 | tf_op jit(solution)/shard_map/dispatch/pallas_call | solution.py:246
  13.6 0.0 copy-done.10
  13.6 11.3 %all-to-all-start = ((bf16[64,8,1024]{2,1,0:T(8,128)(2,1)}), bf16[64,8,1024]{2,1,0:T(8,128)(2,1)S(1)}, u32[]{:S(2)}, u32[]{:S(2)}) async-start(bf16[64,8,1024]{2,1,0:T(8,128)(2,1)} %bitcast.21), calls=%async_computation | async-start | bytes 2097152 | tf_op jit(solution)/shard_map/all_to_all | solution.py:483
  24.8 0.0 copy-start.11
  24.9 0.7 %copy-done.11 = f32[64,128]{1,0:T(8,128)S(1)} copy-done((f32[64,128]{1,0:T(8,128)S(1)}, f32[64,128]{1,0:T(8,128)}, u32[]{:S(2)}) %copy-start.11) | copy-done | bytes 32792
  25.6 3.9 %local.1 = (f32[64,2048]{1,0:T(8,128)S(1)}, bf16[256,512]{1,0:T(8,128)(2,1)S(1)}, bf16[64,64]{1,0:T(8,128)(2,1)}, bf16[64,64]{1,0:T(8,128)(2,1)}) custom-call(bf16[64,2048]{1,0:T(8,128)(2,1)} %get-tuple-element.14.hidden_hbm.hidden_ref, bf16[64,2048]{1,0:T(8,128)(2,1)} %x_hbm.3, bf16[64,2048]{1,0:T(8,128)(2,1)} %bitcast.25, f32[64,128]{1,0:T(8,128)S(1)} %copy-done.11, ...), custom_call_target="tpu_custom_call" | custom-call | flops 4000000000 | bytes 5000000 | tf_op jit(solution)/shard_map/local/pallas_call | solution.py:309
  29.5 0.0 copy-start.2
  29.5 0.8 %copy-done.2 = f32[64,2048]{1,0:T(8,128)} copy-done((f32[64,2048]{1,0:T(8,128)}, f32[64,2048]{1,0:T(8,128)S(1)}, u32[]{:S(2)}) %copy-start.2) | copy-done | bytes 524312
  30.3 0.0 copy-start.6
  30.3 0.7 copy-done.6
  31.0 0.0 copy-start.5
  31.0 0.0 copy-start.9
  31.0 0.0 collective-permute-done.1.gate2_hbm
  31.0 0.0 collective-permute-done.2.up2_hbm
  31.0 0.0 collective-permute-done.3.down2_hbm
  31.0 11.9 %all-to-all-done.rows_ref = bf16[64,8,1024]{2,1,0:T(8,128)(2,1)S(1)} async-done(((bf16[64,8,1024]{2,1,0:T(8,128)(2,1)}), bf16[64,8,1024]{2,1,0:T(8,128)(2,1)S(1)}, u32[]{:S(2)}, u32[]{:S(2)}) %all-to-all-start) | async-done | bytes 1048608 | tf_op jit(solution)/shard_map/all_to_all | solution.py:483
  42.9 0.0 copy-start.3
  42.9 0.0 copy-start.7
  42.9 3.6 %expert.1 = bf16[64,8,1024]{2,1,0:T(8,128)(2,1)S(1)} custom-call(bf16[64,64]{1,0:T(8,128)(2,1)} %get-tuple-element.11.order_ref, bf16[64,8,1024]{2,1,0:T(8,128)(2,1)S(1)} %all-to-all-done.rows_ref, bf16[2048,256]{1,0:T(8,128)(2,1)S(1)} %bitcast.16, bf16[2048,256]{1,0:T(8,128)(2,1)S(1)} %bitcast.18, bf16[256,2048]{1,0:T(8,128)(2,1)} %bitcast.11.down_hbm, ...), custom_call_target="tpu_custom_call" | custom-call | flops 2000000000 | bytes 8000000 | tf_op jit(solution)/shard_map/expert/pallas_call | solution.py:388
  46.5 21.0 %all_to_all.10 = bf16[64,8,1024]{2,1,0:T(8,128)(2,1)S(1)} all-to-all(bf16[64,8,1024]{2,1,0:T(8,128)(2,1)S(1)} %expert.1), channel_id=1, replica_groups=mesh['ep'=64,'tp'=2] {'ep'}, dimensions={0} | all-to-all | bytes 2097152 | tf_op jit(solution)/shard_map/all_to_all | solution.py:493
  67.5 0.0 copy-done.5
  67.5 0.0 copy-done.3
  67.5 0.0 copy-done.7
  67.5 0.4 combine.1
  67.9 3.2 %collective-permute-start.4 = (bf16[128,1024]{1,0:T(8,128)(2,1)S(1)}, bf16[128,1024]{1,0:T(8,128)(2,1)S(1)}, u32[]{:S(2)}, u32[]{:S(2)}) collective-permute-start(bf16[128,1024]{1,0:T(8,128)(2,1)S(1)} %get-tuple-element.21), channel_id=1, source_target_pairs={{0,1},{1,0},{2,3},{3,2},{4,5},{5,4},{6,7},{7,6},{8,9},{9,8},{10,11... | collective-permute-start | bytes 786440 | tf_op jit(solution)/shard_map/ppermute | solution.py:44
  71.2 1.2 %collective-permute-done.4.other_ref = bf16[128,1024]{1,0:T(8,128)(2,1)S(1)} collective-permute-done((bf16[128,1024]{1,0:T(8,128)(2,1)S(1)}, bf16[128,1024]{1,0:T(8,128)(2,1)S(1)}, u32[]{:S(2)}, u32[]{:S(2)}) %collective-permute-start.4) | collective-permute-done | bytes 262176 | tf_op jit(solution)/shard_map/ppermute | solution.py:44
  72.3 0.0 copy-done.9
  72.4 0.9 %finish.1 = bf16[64,1024]{1,0:T(8,128)(2,1)} custom-call(s32[1]{0:T(128)} %bitcast.core_ref, f32[128,1024]{1,0:T(8,128)S(1)} %get-tuple-element.20.mine_ref, bf16[128,1024]{1,0:T(8,128)(2,1)S(1)} %collective-permute-done.4.other_ref, f32[1,1024]{1,0:T(1,128)S(1)} %bitcast.20), custom_call_target="tpu_custom_call" | custom-call | flops 10000000 | bytes 2000000 | tf_op jit(solution)/shard_map/finish/pallas_call | solution.py:440
Async XLA Ops:
  0.6 10.2 %copy-start = (bf16[1,2048,256]{2,1,0:T(8,128)(2,1)S(1)}, bf16[1,2048,256]{2,1,0:T(8,128)(2,1)}, u32[]{:S(2)}) copy-start(bf16[1,2048,256]{2,1,0:T(8,128)(2,1)} %param.31) | copy-start | bytes 3145732
  0.6 10.3 %copy-start.1 = (bf16[1,2048,256]{2,1,0:T(8,128)(2,1)S(1)}, bf16[1,2048,256]{2,1,0:T(8,128)(2,1)}, u32[]{:S(2)}) copy-start(bf16[1,2048,256]{2,1,0:T(8,128)(2,1)} %param.32) | copy-start | bytes 3145732
  0.7 10.8 %copy-start.12 = (s32[64,4]{0,1:T(4,128)S(1)}, s32[64,4]{0,1:T(4,128)}, u32[]{:S(2)}) copy-start(s32[64,4]{0,1:T(4,128)} %param.30) | copy-start | bytes 3076
  0.7 11.4 %copy-start.4 = (bf16[64,2048]{1,0:T(8,128)(2,1)S(1)}, bf16[64,2048]{1,0:T(8,128)(2,1)}, u32[]{:S(2)}) copy-start(bf16[64,2048]{1,0:T(8,128)(2,1)} %x_hbm.3) | copy-start | bytes 786436
  0.7 11.4 %copy-start.8 = (f32[2048]{0:T(1024)S(1)}, f32[2048]{0:T(1024)}, u32[]{:S(2)}) copy-start(f32[2048]{0:T(1024)} %param.28) | copy-start | bytes 24580
  9.4 2.6 %collective-permute-start = (bf16[64,2048]{1,0:T(8,128)(2,1)S(1)}, bf16[64,2048]{1,0:T(8,128)(2,1)S(1)}, u32[]{:S(2)}, u32[]{:S(2)}) collective-permute-start(bf16[64,2048]{1,0:T(8,128)(2,1)S(1)} %attend.1.own_ref), channel_id=1, source_target_pairs={{0,1},{1,0},{2,3},{3,2},{4,5},{5,4},{6,7},{7,6},{8,9},{9,8},{10,11... | collective-permute-start | bytes 786440 | tf_op jit(solution)/shard_map/ppermute | solution.py:44
  10.9 20.1 %collective-permute-start.1 = (bf16[2048,256]{1,0:T(8,128)(2,1)S(1)}, bf16[2048,256]{1,0:T(8,128)(2,1)}, u32[]{:S(2)}, u32[]{:S(2)}) collective-permute-start(bf16[2048,256]{1,0:T(8,128)(2,1)S(1)} %bitcast.15), channel_id=1, source_target_pairs={{0,1},{1,0},{2,3},{3,2},{4,5},{5,4},{6,7},{7,6},{8,9},{9,8},{10,11... | collective-permute-start | bytes 3145736 | tf_op jit(solution)/shard_map/ppermute | solution.py:44
  11.0 20.0 %collective-permute-start.2 = (bf16[2048,256]{1,0:T(8,128)(2,1)S(1)}, bf16[2048,256]{1,0:T(8,128)(2,1)}, u32[]{:S(2)}, u32[]{:S(2)}) collective-permute-start(bf16[2048,256]{1,0:T(8,128)(2,1)S(1)} %bitcast.17), channel_id=1, source_target_pairs={{0,1},{1,0},{2,3},{3,2},{4,5},{5,4},{6,7},{7,6},{8,9},{9,8},{10,11... | collective-permute-start | bytes 3145736 | tf_op jit(solution)/shard_map/ppermute | solution.py:44
  11.4 19.6 %collective-permute-start.3 = (bf16[256,2048]{1,0:T(8,128)(2,1)}, bf16[256,2048]{1,0:T(8,128)(2,1)}, u32[]{:S(2)}, u32[]{:S(2)}) collective-permute-start(bf16[256,2048]{1,0:T(8,128)(2,1)} %bitcast.11.down_hbm), channel_id=1, source_target_pairs={{0,1},{1,0},{2,3},{3,2},{4,5},{5,4},{6,7},{7,6},{8,9},{9,8},{10,11... | collective-permute-start | bytes 3145736 | tf_op jit(solution)/shard_map/ppermute | solution.py:44
  11.9 1.7 %copy-start.10 = (f32[64,128]{1,0:T(8,128)}, f32[64,128]{1,0:T(8,128)S(1)}, u32[]{:S(2)}) copy-start(f32[64,128]{1,0:T(8,128)S(1)} %get-tuple-element.15.member_ref) | copy-start | bytes 98308
  13.6 29.4 %all-to-all-start = ((bf16[64,8,1024]{2,1,0:T(8,128)(2,1)}), bf16[64,8,1024]{2,1,0:T(8,128)(2,1)S(1)}, u32[]{:S(2)}, u32[]{:S(2)}) async-start(bf16[64,8,1024]{2,1,0:T(8,128)(2,1)} %bitcast.21), calls=%async_computation | async-start | bytes 2097152 | tf_op jit(solution)/shard_map/all_to_all | solution.py:483
  24.8 0.8 %copy-start.11 = (f32[64,128]{1,0:T(8,128)S(1)}, f32[64,128]{1,0:T(8,128)}, u32[]{:S(2)}) copy-start(f32[64,128]{1,0:T(8,128)} %copy-done.10) | copy-start | bytes 98308
  29.5 0.8 %copy-start.2 = (f32[64,2048]{1,0:T(8,128)}, f32[64,2048]{1,0:T(8,128)S(1)}, u32[]{:S(2)}) copy-start(f32[64,2048]{1,0:T(8,128)S(1)} %get-tuple-element.19.shared_ref) | copy-start | bytes 1572868
  30.3 0.7 copy-start.6
  31.0 36.5 %copy-start.5 = (bf16[64,2048]{1,0:T(8,128)(2,1)S(1)}, bf16[64,2048]{1,0:T(8,128)(2,1)}, u32[]{:S(2)}) copy-start(bf16[64,2048]{1,0:T(8,128)(2,1)} %get-tuple-element.14.hidden_hbm.hidden_ref) | copy-start | bytes 786436
  31.0 41.4 %copy-start.9 = (f32[1024]{0:T(1024)S(1)}, f32[1024]{0:T(1024)}, u32[]{:S(2)}) copy-start(f32[1024]{0:T(1024)} %param.37) | copy-start | bytes 12292
  42.9 24.6 %copy-start.3 = (f32[64,2048]{1,0:T(8,128)S(1)}, f32[64,2048]{1,0:T(8,128)}, u32[]{:S(2)}) copy-start(f32[64,2048]{1,0:T(8,128)} %copy-done.2) | copy-start | bytes 1572868
  42.9 24.6 %copy-start.7 = (bf16[256,512]{1,0:T(8,128)(2,1)S(1)}, bf16[256,512]{1,0:T(8,128)(2,1)}, u32[]{:S(2)}) copy-start(bf16[256,512]{1,0:T(8,128)(2,1)} %copy-done.6) | copy-start | bytes 786436
  67.9 4.4 %collective-permute-start.4 = (bf16[128,1024]{1,0:T(8,128)(2,1)S(1)}, bf16[128,1024]{1,0:T(8,128)(2,1)S(1)}, u32[]{:S(2)}, u32[]{:S(2)}) collective-permute-start(bf16[128,1024]{1,0:T(8,128)(2,1)S(1)} %get-tuple-element.21), channel_id=1, source_target_pairs={{0,1},{1,0},{2,3},{3,2},{4,5},{5,4},{6,7},{7,6},{8,9},{9,8},{10,11... | collective-permute-start | bytes 786440 | tf_op jit(solution)/shard_map/ppermute | solution.py:44
